TPU v7x, 256 devices: a whole 4x4x8 slice. The times are simulated.
256 devices in a mesh: fs: 64 (over z, y, core), tp: 4 (over x).
Axes of the slice: x: 4, y: 4, z: 8, core: 2. Of those that a mesh axis runs over, the one named last changes fastest.
Arguments:
- tokens: bfloat16 [3072, 2048], P('tp'), may hold values from -6 to 6
- norm_gain: float32 [2048], P('fs'), may hold values from 0.1 to 1.9
- gate_weight: float32 [4, 2048, 8192], P(None, 'fs', 'tp'), may hold values from -0.125 to 0.125
- up_weight: float32 [4, 2048, 8192], P(None, 'fs', 'tp'), may hold values from -0.125 to 0.125
- down_weight: float32 [4, 8192, 2048], P(None, 'fs', 'tp'), may hold values from -0.0625 to 0.0625
- routes: int32 [3072, 2], P('tp'), may hold values from 0 to 3, all different within a row; in each aligned block of 768 rows (0 to 767, 768 to 1535, ...) at most 480 rows name the same one
- route_logit: float32 [3072, 2], P('tp'), may hold values from -6 to 6
Outputs:
- gate_out: bfloat16 [4, 2048, 8192], P(None, None, 'fs')
- up_out: bfloat16 [4, 2048, 8192], P(None, None, 'fs')
- down_out: bfloat16 [4, 8192, 2048], P(None, 'fs')
- mixed: bfloat16 [3072, 2048], P(('tp', 'fs'))
Inputs may be any that keep to these rules, and one draw needn't show every extreme that they name: `routes`: the two experts of a token differ. In each aligned block of 768 tokens (the tokens of one request group) every expert is named by at most 480 tokens, a bound that some block reaches.
All inputs are finite; a program needn't handle non-finite values.
Results may differ from a plain program's by a relative error of at most 0.0082.
Values may be sent and summed in bfloat16 or wider, within the bound.
A program may use at most 128 MiB of HBM per device.

v0:
```python
import jax
import jax.numpy as jnp
from jax import lax
from jax.sharding import Mesh
from jax.sharding import PartitionSpec as P

FS = ("fs_0", "fs_1", "fs_2")
TP_FS = ("tp", "fs_0", "fs_1", "fs_2")


EPS = 0.5


def in_one_piece(arrays, axis, split_dim, concat_dim, along):
    widths = [a.shape[along] for a in arrays]
    both = jnp.concatenate(arrays, axis=along)
    whole = lax.all_to_all(both, axis, split_axis=split_dim, concat_axis=concat_dim, tiled=True)
    return tuple(jnp.split(whole, [sum(widths[:k]) for k in range(1, len(widths))], axis=along))


def sent_together(arrays, axis, dim, along):
    widths = [a.shape[along] for a in arrays]
    both = jnp.concatenate(arrays, axis=along)
    whole = lax.all_gather(both, axis, axis=dim, tiled=True)
    return tuple(jnp.split(whole, [sum(widths[:k]) for k in range(1, len(widths))], axis=along))


def laid_out(parts, dim):
    lengths = list(parts.shape[1:])
    lengths[dim] *= parts.shape[0]
    return jnp.moveaxis(parts, 0, dim).reshape(lengths)


def copy_for_each(shard, axis):
    copies = jnp.broadcast_to(shard, (lax.axis_size(axis), *shard.shape))
    return lax.all_to_all(copies, axis, split_axis=0, concat_axis=0, tiled=True)


def gather_directly(shard, axis, dim):
    return laid_out(copy_for_each(shard, axis), dim)


def sum_by_axis(so_far, axes):
    for axis in axes:
        so_far = lax.psum_scatter(so_far, axis, scatter_dimension=0, tiled=True)
    return so_far


def shards(tokens, norm_gain, gate_weight, up_weight, down_weight, routes, route_logit):
    gain_col = norm_gain[None, :, None]
    gate_part = (gate_weight * gain_col).astype(jnp.bfloat16)
    up_part = (up_weight * gain_col).astype(jnp.bfloat16)
    down_part = down_weight.astype(jnp.bfloat16)
    gate_one, up_one = in_one_piece((gate_part, up_part), "tp", 0, 2, 1)
    gate_mine, up_mine = in_one_piece((gate_one, up_one), FS, 2, 1, 0)
    gate_out, up_out = sent_together((gate_mine, up_mine), "tp", 0, 1)
    down_out = gather_directly(down_part, "tp", 2)
    total_rows = tokens.shape[0]
    width = tokens.shape[1]
    experts = gate_out.shape[0]
    capacity = total_rows * 5 // 8
    floats = tokens.astype(jnp.float32)
    normed = (floats * lax.rsqrt(jnp.mean(floats * floats, axis=1, keepdims=True) + EPS)).astype(
        jnp.bfloat16
    )
    first_share = jax.nn.sigmoid(route_logit[:, 0] - route_logit[:, 1])
    shares = jnp.stack([first_share, 1.0 - first_share], axis=1)
    chosen = (routes[:, :, None] == jnp.arange(experts, dtype=jnp.int32)[None, None, :]).astype(
        jnp.int32
    )
    counts = jnp.sum(chosen, axis=1)
    before = jnp.cumsum(counts, axis=0) - counts
    slot_index = jnp.sum(chosen * before[:, None, :], axis=2)
    flat_slot = routes * capacity + slot_index
    row_ids = jnp.repeat(jnp.arange(total_rows, dtype=jnp.int32), 2)
    table = (
        jnp.full((experts * capacity,), total_rows, jnp.int32)
        .at[flat_slot.reshape(-1)]
        .set(row_ids)
    )
    gathered = jnp.take(normed, table, axis=0, mode="fill", fill_value=0).reshape(
        experts, capacity, width
    )
    gate_val = jnp.einsum("ecd,edf->ecf", gathered, gate_out, preferred_element_type=jnp.float32)
    up_val = jnp.einsum("ecd,edf->ecf", gathered, up_out, preferred_element_type=jnp.float32)
    hidden = (jax.nn.silu(gate_val) * up_val).astype(jnp.bfloat16)
    results = jnp.einsum("ecf,efd->ecd", hidden, down_out, preferred_element_type=jnp.float32)
    flat_rows = results.reshape(experts * capacity, width)
    first_rows = jnp.take(flat_rows, flat_slot[:, 0], axis=0)
    second_rows = jnp.take(flat_rows, flat_slot[:, 1], axis=0)
    mixed = sum_by_axis(shares[:, 0:1] * first_rows + shares[:, 1:2] * second_rows, FS)
    return (gate_out, up_out, down_out, mixed.astype(jnp.bfloat16))


def solution(mesh):
    finer = Mesh(mesh.devices.reshape(8, 4, 2, mesh.shape["tp"]), ("fs_0", "fs_1", "fs_2", "tp"))
    in_specs = (
        P("tp", None),
        P(FS),
        P(None, FS, "tp"),
        P(None, FS, "tp"),
        P(None, FS, "tp"),
        P("tp", None),
        P("tp", None),
    )
    out_specs = (P(None, None, FS), P(None, None, FS), P(None, FS, None), P(TP_FS, None))
    return jax.shard_map(
        shards, mesh=finer, in_specs=in_specs, out_specs=out_specs, check_vma=False
    )
```

profile of v0, /device:TPU:1, one launch (start us, length us, event | category | flops | bytes accessed | tf_op | source)
XLA Modules:
  0.0 327.9 jit_solution(8759569228513904316)
XLA Ops:
  7.2 0.0 all-gather.2.cloned.1.call-start
  7.2 1.8 multiply_convert_fusion.1
  9.0 0.1 pad_maximum_fusion
  9.1 18.8 %all_to_all.38 = bf16[4,64,2048]{2,1,0:T(8,128)(2,1)S(1)} all-to-all(bf16[4,64,2048]{2,1,0:T(8,128)(2,1)S(1)} %pad_maximum_fusion), channel_id=1, replica_groups=mesh['fs_0'=8,'fs_1'=4,'fs_2'=2,'tp'=4] {'tp'}, dimensions={0} | all-to-all | bytes 2097152 | tf_op jit(solution)/shard_map/all_to_all | solution.py:17
  28.0 0.1 copy.43
  28.0 0.1 fusion.28
  28.1 0.1 pad_maximum_fusion.1
  28.2 6.8 %copy.36 = bf16[2,32,8192]{1,0,2:T(2,128)(2,1)} copy(bf16[2,32,8192]{2,1,0:T(8,128)(2,1)S(1)} %pad_maximum_fusion.1) | data formatting | bytes 2097152 | tf_op jit(solution)/shard_map/concatenate | solution.py:16
  35.0 9.1 %reshape.142 = bf16[64,2,4096]{2,1,0:T(2,128)(2,1)S(1)} reshape(bf16[8192,2,32]{2,1,0:T(2,128)(2,1)} %bitcast.38) | data formatting | bytes 2097152
  44.2 41.5 %all_to_all.39 = bf16[64,2,4096]{2,1,0:T(2,128)(2,1)S(1)} all-to-all(bf16[64,2,4096]{2,1,0:T(2,128)(2,1)S(1)} %reshape.142), channel_id=1, replica_groups=mesh['fs_0'=8,'fs_1'=4,'fs_2'=2,'tp'=4] {'fs_0','fs_1','fs_2'}, dimensions={0} | all-to-all | bytes 2097152 | tf_op jit(solution)/shard_map/all_to_all | solution.py:17
  85.6 3.5 %reshape.143 = bf16[8192,2,32]{2,1,0:T(2,128)(2,1)} reshape(bf16[64,2,4096]{2,1,0:T(2,128)(2,1)S(1)} %all_to_all.39) | data formatting | bytes 2097152
  89.2 6.1 %copy.42 = bf16[2,32,64,128]{3,2,1,0:T(8,128)(2,1)S(1)} copy(bf16[2,32,64,128]{1,0,3,2:T(2,128)(2,1)} %bitcast.39) | data formatting | bytes 2097152 | tf_op jit(solution)/shard_map/all_to_all | solution.py:17
  95.3 0.1 fusion.27
  95.3 0.3 copy.38
  95.7 0.0 copy-start.4
  95.7 0.3 copy.39
  96.0 0.0 copy-start.1
  96.1 1.0 pad_maximum_fusion.2
  97.1 0.0 all-gather.2.cloned.1.call-update
  97.1 1.5 convert_element_type.26
  98.7 1.5 broadcast_in_dim.38
  100.2 4.4 %all-to-all-start.2 = ((bf16[4,4,128,512]{3,2,1,0:T(8,128)(2,1)}), bf16[4,4,128,512]{3,2,1,0:T(8,128)(2,1)}, u32[]{:S(2)}, u32[]{:S(2)}) async-start(bf16[4,4,128,512]{3,2,1,0:T(8,128)(2,1)} %broadcast_in_dim.38), calls=%async_computation.2 | async-start | bytes 4194304 | tf_op jit(solution)/shard_map/all_to_all | solution.py:36
  104.7 0.0 reduce-scatter.5.cloned.1.call-start
  104.7 0.0 copy-done.4
  104.7 1.1 reduce-window.6
  105.9 0.2 slice_reduce_fusion
  106.1 0.2 reduce-window.9
  106.3 0.1 add_bitcast_fusion
  106.4 0.2 copy.41
  106.6 0.3 reshape.91
  106.9 0.8 reshape.122
  107.8 6.5 %scatter_custom_fusion = s32[1920]{0:T(1024)S(1)} fusion(s32[1536]{0:T(1024)S(1)} %fusion.18, s32[1536]{0:T(1024)} %reshape.122, s32[]{:T(128)} %constant.23.clone.1), kind=kCustom, calls=%fused_computation.49 | custom fusion | bytes 8192 | tf_op jit(solution)/shard_map/scatter | solution.py:79
  114.3 0.1 broadcast_in_dim.41
  114.4 0.0 copy-done.1
  114.4 0.7 fusion.3
  115.1 2.5 fusion.4
  117.7 0.0 copy-start.5
  117.7 8.8 %gather_fusion = bf16[1920,2048]{1,0:T(8,128)(2,1)} fusion(bf16[768,2048]{1,0:T(8,128)(2,1)S(1)} %fusion.4, s32[2048]{0:T(1024)S(1)} %pad_clamp_fusion), kind=kCustom, calls=%fused_computation.2 | custom fusion | bytes 15736320 | tf_op jit(solution)/shard_map/jit(_take)/gather | solution.py:81
  126.5 0.0 copy-done.5
  126.6 25.4 %all-to-all-done.2 = bf16[4,4,128,512]{3,2,1,0:T(8,128)(2,1)} async-done(((bf16[4,4,128,512]{3,2,1,0:T(8,128)(2,1)}), bf16[4,4,128,512]{3,2,1,0:T(8,128)(2,1)}, u32[]{:S(2)}, u32[]{:S(2)}) %all-to-all-start.2) | async-done | bytes 2097184 | tf_op jit(solution)/shard_map/all_to_all | solution.py:36
  152.0 1.9 copy.44
  153.8 0.0 copy-start.2
  153.9 11.2 %all-gather.2.cloned.1.call-done = bf16[4,4096,128]{2,1,0:T(8,128)(2,1)} async-done(((bf16[1,4096,128]{2,1,0:T(8,128)(2,1)}), bf16[4,4096,128]{2,1,0:T(8,128)(2,1)}) %all-gather.2.cloned.1.call-update) | async-done | bytes 4194320 | tf_op jit(solution)/shard_map/all_gather | solution.py:24
  165.0 4.0 %fusion.26 = (bf16[4,2048,128]{2,1,0:T(8,128)(2,1)}, bf16[4,2048,128]{2,1,0:T(8,128)(2,1)S(1)}) fusion(bf16[4,4096,128]{2,1,0:T(8,128)(2,1)} %all-gather.2.cloned.1.call-done), kind=kLoop, calls=%fused_computation.61 | loop fusion | bytes 8388608 | tf_op jit(solution)/shard_map/split | solution.py:25
  169.0 1.9 copy-done
  170.9 2.5 fusion.2
  173.4 0.0 copy-done.3
  173.4 0.0 copy-done.2
  173.4 10.2 %fusion.10 = f32[4,480,2048]{2,1,0:T(8,128)} fusion(bf16[4,128,2048]{2,1,0:T(8,128)(2,1)S(1)} %bitcast.40, bf16[4,2048,128]{2,1,0:T(8,128)(2,1)} %get-tuple-element.9, bf16[4,480,2048]{2,1,0:T(8,128)(2,1)} %bitcast.36, pred[4,480]{1,0:T(4,128)(4,1)S(1)} %broadcast_in_dim.41, f32[4,480,128]{2,1,0:T(8,128)S(1)} %fusion.2), kind=kOutput, calls=%fused_computation.18 | convolution fusion | flops 2018672640 | bytes 28772224 | tf_op jit(solution)/shard_map/ecf,efd->ecd/dot_general | solution.py:87
  183.6 12.7 %gather_fusion.1 = f32[768,2048]{1,0:T(8,128)} fusion(f32[1920,2048]{1,0:T(8,128)} %bitcast.34, s32[1024]{0:T(1024)S(1)} %pad_clamp_fusion.2), kind=kCustom, calls=%fused_computation.clone | custom fusion | bytes 12585984 | tf_op jit(solution)/shard_map/jit(_take)/gather | solution.py:89
  196.3 12.6 %gather_fusion.2 = f32[768,2048]{1,0:T(8,128)} fusion(f32[1920,2048]{1,0:T(8,128)} %bitcast.35, s32[1024]{0:T(1024)S(1)} %pad_clamp_fusion.1), kind=kCustom, calls=%fused_computation.1.clone | custom fusion | bytes 12585984 | tf_op jit(solution)/shard_map/jit(_take)/gather | solution.py:90
  209.0 7.3 %fusion.5 = f32[768,2048]{1,0:T(8,128)} fusion(f32[768,2048]{1,0:T(8,128)} %gather_fusion.2, f32[768,2048]{1,0:T(8,128)} %gather_fusion.1, f32[768]{0:T(1024)S(1)} %get-tuple-element.8, f32[768]{0:T(1024)S(1)} %get-tuple-element.7, pred[768]{0:T(1024)(128)(4,1)S(1)} %get-tuple-element.19, pred[768]{0:T(1024)(128)(4,1)S(1)} %get-tuple-element.20), kind=kLoop, calls=%fused_computation.12 | loop fusion | flops 7864320 | bytes 18882048 | tf_op jit(solution)/shard_map/add | solution.py:91
  216.3 0.0 reduce-scatter.5.cloned.1.call-update
  216.3 0.0 reduce-scatter.7.cloned.1.call-start
  216.4 70.2 %reduce-scatter.5.cloned.1.call-done = f32[96,2048]{1,0:T(8,128)} async-done(((f32[768,2048]{1,0:T(8,128)}), f32[96,2048]{1,0:T(8,128)}) %reduce-scatter.5.cloned.1.call-update) | async-done | bytes 786448 | tf_op jit(solution)/shard_map/reduce_scatter | solution.py:45
  286.6 0.0 reduce-scatter.7.cloned.1.call-update
  286.7 24.3 %reduce-scatter.7.cloned.1.call-done = f32[24,2048]{1,0:T(8,128)} async-done(((f32[96,2048]{1,0:T(8,128)}), f32[24,2048]{1,0:T(8,128)}) %reduce-scatter.7.cloned.1.call-update) | async-done | bytes 196624 | tf_op jit(solution)/shard_map/reduce_scatter | solution.py:45
  310.9 6.5 %fusion = f32[16,2048]{1,0:T(8,128)S(1)} fusion(f32[24,2048]{1,0:T(8,128)} %reduce-scatter.7.cloned.1.call-done), kind=kCustom, calls=%all-reduce-scatter | all-reduce-scatter fusion | flops 65537 | bytes 328704
  317.5 1.3 collective-permute-start
  318.8 0.0 copy-done.6
  318.8 0.6 dynamic-slice.4
  320.0 0.5 collective-permute-done
  320.5 0.2 concatenate.12
  320.8 0.7 dynamic-slice_convert_fusion
  (21 shorter events, 0.3 us)
Async XLA Ops:
  7.2 157.9 %all-gather.2.cloned.1.call-start = ((), (), s32[]{:S(2)}) async-start(), calls=%async_computation.5 | async-start | bytes 5242880 | tf_op jit(solution)/shard_map/all_gather | solution.py:24
  95.7 9.0 %copy-start.4 = (s32[768,2]{0,1:T(2,128)S(1)}, s32[768,2]{0,1:T(2,128)}, u32[]{:S(2)}) copy-start(s32[768,2]{0,1:T(2,128)} %param.14) | copy-start | bytes 18436
  96.0 18.4 %copy-start.1 = (bf16[768,2048]{1,0:T(8,128)(2,1)S(1)}, bf16[768,2048]{1,0:T(8,128)(2,1)}, u32[]{:S(2)}) copy-start(bf16[768,2048]{1,0:T(8,128)(2,1)} %param.9) | copy-start | bytes 9437188
  100.2 51.8 %all-to-all-start.2 = ((bf16[4,4,128,512]{3,2,1,0:T(8,128)(2,1)}), bf16[4,4,128,512]{3,2,1,0:T(8,128)(2,1)}, u32[]{:S(2)}, u32[]{:S(2)}) async-start(bf16[4,4,128,512]{3,2,1,0:T(8,128)(2,1)} %broadcast_in_dim.38), calls=%async_computation.2 | async-start | bytes 4194304 | tf_op jit(solution)/shard_map/all_to_all | solution.py:36
  104.7 182.0 %reduce-scatter.5.cloned.1.call-start = ((), (), s32[]{:S(2)}) async-start(), calls=%async_computation.6 | async-start | bytes 7077888 | tf_op jit(solution)/shard_map/reduce_scatter | solution.py:45
  117.7 8.8 %copy-start.5 = (f32[768,2]{0,1:T(2,128)S(1)}, f32[768,2]{0,1:T(2,128)}, u32[]{:S(2)}) copy-start(f32[768,2]{0,1:T(2,128)} %param.15) | copy-start | bytes 18436
  153.8 19.6 %copy-start.2 = (bf16[4,4,16,8,512]{4,3,0,2,1:T(8,128)(2,1)}, bf16[4,4,16,8,512]{4,3,0,2,1:T(8,128)(2,1)S(1)}, u32[]{:S(2)}) copy-start(bf16[4,4,16,8,512]{4,3,0,2,1:T(8,128)(2,1)S(1)} %copy.44) | copy-start | bytes 6291460
  165.0 5.9 %copy-start = (bf16[1920,2048]{1,0:T(8,128)(2,1)S(1)}, bf16[1920,2048]{1,0:T(8,128)(2,1)}, u32[]{:S(2)}) copy-start(bf16[1920,2048]{1,0:T(8,128)(2,1)} %gather_fusion) | copy-start | bytes 23592964
  169.0 4.4 %copy-start.3 = (bf16[4,2048,128]{2,1,0:T(8,128)(2,1)}, bf16[4,2048,128]{2,1,0:T(8,128)(2,1)S(1)}, u32[]{:S(2)}) copy-start(bf16[4,2048,128]{2,1,0:T(8,128)(2,1)S(1)} %get-tuple-element.10) | copy-start | bytes 6291460
  216.3 102.4 %copy-start.6 = (u32[256]{0:T(256)S(1)}, u32[256]{0:T(256)}, u32[]{:S(2)}) copy-start(u32[256]{0:T(256)} %constant.53) | copy-start | bytes 3076
  216.3 94.6 %reduce-scatter.7.cloned.1.call-start = ((), (), s32[]{:S(2)}) async-start(), calls=%async_computation.7 | async-start | bytes 983040 | tf_op jit(solution)/shard_map/reduce_scatter | solution.py:45
  317.5 3.1 collective-permute-start
Sparse Core Ops, SparseCore 0:
  97.2 67.7 all-gather.1
  216.5 70.1 reduce-scatter.4
  289.2 21.6 reduce-scatter.6
where the time goes:
time: 329 us; the launch traced here: 328 us
  waiting for transfers between devices  132 us (40%)
  local copies, waits for them, and re-layouts  79.5 us (24%)
  blocking collectives  66.8 us (20%)
  other arithmetic  16.7 us (5%)
  between operations  14.7 us (4%)
  matrix products  12.7 us (4%)
  starting transfers between devices  5.86 us (2%)
    reduce_scatter x2, waiting for transfers between devices, sum_by_axis(): so_far = lax.psum_scatter(so_far, axis, scatter_dimension=0, tiled=True)  94.5 us
    all_to_all x2, blocking collectives, in_one_piece(): lax.all_to_all(both, axis, split_axis=split_dim, concat_axis=concat_dim,...  60.3 us
    all_to_all x1, waiting for transfers between devices, copy_for_each(): return lax.all_to_all(copies, axis, split_axis=0, concat_axis=0, tiled=True)  25.4 us
    unnamed x19, local copies, waits for them, and re-layouts  15.4 us
    gather x1, local copies, waits for them, and re-layouts, shards(): first_rows = jnp.take(flat_rows, flat_slot[:, 0], axis=0)  12.7 us
    gather x1, local copies, waits for them, and re-layouts, shards(): second_rows = jnp.take(flat_rows, flat_slot[:, 1], axis=0)  12.6 us
    all_gather x1, waiting for transfers between devices, sent_together(): whole = lax.all_gather(both, axis, axis=dim, tiled=True)  11.2 us
    dot_general x1, matrix products, shards(): jnp.einsum('ecf,efd->ecd', hidden, down_out, preferred_element_type=jnp.f...  10.2 us
  transfers between devices with their start and end apart: 5, of which 5 were waited for; matrix products, arithmetic and copies ran while one was open for 8% of the time, Pallas kernels for 0%

commit v1 on v0

v1 whole, which is shorter than its diff:
```python
import functools

import jax
import jax.numpy as jnp
from jax import lax
from jax.experimental import pallas as pl
from jax.experimental.pallas import tpu as pltpu
from jax.sharding import Mesh
from jax.sharding import PartitionSpec as P

FS = ("fs_0", "fs_1", "fs_2")
TP_FS = ("tp", "fs_0", "fs_1", "fs_2")
EPS = 0.5
MESH = pl.DeviceIdType.MESH


def weights_kernel(
    sizes,
    gate_ref,
    up_ref,
    gain_ref,
    down_ref,
    gate_out,
    up_out,
    down_out,
    staged,
    spread,
    by_z,
    a_send,
    a_recv,
    z_send,
    z_recv,
    y_send,
    y_recv,
    c_send,
    c_recv,
    f_send,
    f_recv,
):
    nz, ny, nc, nx = sizes
    nyc = ny * nc
    nk = nz * nyc
    per_x = nk // nx
    my_z, my_y = lax.axis_index("fs_0"), lax.axis_index("fs_1")
    my_c, my_x = lax.axis_index("fs_2"), lax.axis_index("tp")
    my_yc = my_y * nc + my_c
    outs = (gate_out, up_out)

    def at(dz=0, dy=0, dc=0, dx=0):
        return (
            lax.rem(my_z + dz, nz),
            lax.rem(my_y + dy, ny),
            lax.rem(my_c + dc, nc),
            lax.rem(my_x + dx, nx),
        )

    yc_steps = [(dy, dc) for dy in range(ny) for dc in range(nc) if dy + dc > 0]
    peers = (
        [at(dx=d) for d in range(1, nx)]
        + [at(dz=d) for d in range(1, nz)]
        + [at(dy=dy, dc=dc) for dy, dc in yc_steps]
    )
    barrier = pltpu.get_barrier_semaphore()
    for peer in peers:
        pl.semaphore_signal(barrier, inc=1, device_id=peer, device_id_type=MESH)

    def remote(src, dst, ssem, rsem, peer):
        return pltpu.make_async_remote_copy(
            src_ref=src, dst_ref=dst, send_sem=ssem, recv_sem=rsem, device_id=peer, device_id_type=MESH
        )

    rows = gate_ref.shape[1]
    width = gate_ref.shape[2] // per_x
    gain = gain_ref[...]

    def convert(m, ref):
        for d in range(nx):
            expert = lax.rem(my_x + d, nx)
            for k in range(per_x):
                block = (ref[expert, :, k * width : (k + 1) * width] * gain).astype(jnp.bfloat16)
                if d == 0:
                    spread[m, my_x * per_x + k] = block
                else:
                    staged[m, d, k] = block

    sent = []

    def start(copy):
        copy.start()
        sent.append(copy)
        return copy

    a_copies = {}
    for m, ref in ((0, gate_ref), (1, up_ref)):
        convert(m, ref)
        if m == 0:
            pl.semaphore_wait(barrier, len(peers))
        for d in range(1, nx):
            a_copies[m, d] = start(
                remote(
                    staged.at[m, d],
                    spread.at[m, pl.ds(my_x * per_x, per_x)],
                    a_send.at[m, d],
                    a_recv.at[m, d],
                    at(dx=d),
                )
            )
    cols = down_ref.shape[2]
    half_e = nx // 2
    own = pl.ds(pl.multiple_of(my_x * cols, cols), cols)
    for e in range(nx):
        down_out[e, :, own] = down_ref[e].astype(jnp.bfloat16)

    def ring(tag, block):
        near = {}
        for h in (0, 1):
            near[0, h] = start(
                remote(
                    block(my_x, h), block(my_x, h), c_send.at[tag, 0, h], c_recv.at[tag, 0, h], at(dx=1)
                )
            )
            g = 1 - h
            near[1, g] = start(
                remote(
                    block(my_x, g), block(my_x, g), c_send.at[tag, 1, g], c_recv.at[tag, 1, g], at(dx=nx - 1)
                )
            )
        return near

    def pass_on(tag, block, near):
        left, right = lax.rem(my_x + nx - 1, nx), lax.rem(my_x + 1, nx)
        near[0, 0].wait_recv()
        first = start(
            remote(block(left, 0), block(left, 0), f_send.at[tag, 0], f_recv.at[tag, 0], at(dx=1))
        )
        near[1, 1].wait_recv()
        second = start(
            remote(block(right, 1), block(right, 1), f_send.at[tag, 1], f_recv.at[tag, 1], at(dx=nx - 1))
        )
        return near[0, 1], near[1, 0], first, second

    def down_block(x, h):
        return down_out.at[
            pl.ds(h * half_e, half_e), :, pl.ds(pl.multiple_of(x * cols, cols), cols)
        ]

    down_near = ring(2, down_block)

    z_copies = {}
    for m in (0, 1):
        for d in range(1, nx):
            a_copies[m, d].wait_recv()
        for dz in range(1, nz):
            peer = at(dz=dz)
            z_copies[m, dz] = start(
                remote(
                    spread.at[m, pl.ds(peer[0] * nyc, nyc)],
                    by_z.at[m, my_z],
                    z_send.at[m, dz],
                    z_recv.at[m, dz],
                    peer,
                )
            )
        by_z[m, my_z] = spread[m, pl.ds(my_z * nyc, nyc)]

    y_copies = {}

    def exchange_yc(m):
        out = outs[m]
        for dz in range(1, nz):
            z_copies[m, dz].wait_recv()
        for i, (dy, dc) in enumerate(yc_steps):
            peer = at(dy=dy, dc=dc)
            y_copies[m, i] = start(
                remote(
                    by_z.at[m, :, peer[1] * nc + peer[2]],
                    out.at[my_x, :, my_yc],
                    y_send.at[m, i],
                    y_recv.at[m, i],
                    peer,
                )
            )
        out[my_x, :, my_yc] = by_z[m, :, my_yc]

    half_z = nz // 2

    def out_block(m):
        return lambda x, h: outs[m].at[x, pl.ds(h * half_z, half_z)]

    exchange_yc(0)
    down_rest = pass_on(2, down_block, down_near)
    for i in range(len(yc_steps)):
        y_copies[0, i].wait_recv()
    near0 = ring(0, out_block(0))
    exchange_yc(1)
    rest0 = pass_on(0, out_block(0), near0)
    for i in range(len(yc_steps)):
        y_copies[1, i].wait_recv()
    near1 = ring(1, out_block(1))
    rest1 = pass_on(1, out_block(1), near1)
    for copy in down_rest + rest0 + rest1:
        copy.wait_recv()
    for copy in sent:
        copy.wait_send()


def hand_over(sizes, gate_weight, up_weight, gain, down_weight):
    nz, ny, nc, nx = sizes
    nyc = ny * nc
    nk = nz * nyc
    per_x = nk // nx
    experts, rows, cols = gate_weight.shape
    width = cols // per_x
    hid, dcols = down_weight.shape[1:]
    bf = jnp.bfloat16
    steps = nyc - 1
    dma = pltpu.SemaphoreType.DMA
    vmem = pl.BlockSpec(memory_space=pltpu.VMEM)
    gate, up, down = pl.pallas_call(
        functools.partial(weights_kernel, sizes),
        out_shape=[
            jax.ShapeDtypeStruct((experts, nz, nyc, rows, width), bf),
            jax.ShapeDtypeStruct((experts, nz, nyc, rows, width), bf),
            jax.ShapeDtypeStruct((experts, hid, dcols * nx), bf),
        ],
        in_specs=[vmem] * 4,
        out_specs=[vmem] * 3,
        scratch_shapes=[
            pltpu.VMEM((2, nx, per_x, rows, width), bf),
            pltpu.VMEM((2, nk, rows, width), bf),
            pltpu.VMEM((2, nz, nyc, rows, width), bf),
            dma((2, nx)),
            dma((2, nx)),
            dma((2, nz)),
            dma((2, nz)),
            dma((2, steps)),
            dma((2, steps)),
            dma((3, 2, 2)),
            dma((3, 2, 2)),
            dma((3, 2)),
            dma((3, 2)),
        ],
        compiler_params=pltpu.CompilerParams(
            collective_id=0, has_side_effects=True, vmem_limit_bytes=60 * 1024 * 1024
        ),
        name="hand_over",
    )(gate_weight, up_weight, gain, down_weight)
    full = (experts, nk * rows, width)
    return gate.reshape(full), up.reshape(full), down


def sum_by_axis(so_far, axes):
    for axis in axes:
        so_far = lax.psum_scatter(so_far, axis, scatter_dimension=0, tiled=True)
    return so_far


def shards(sizes, tokens, norm_gain, gate_weight, up_weight, down_weight, routes, route_logit):
    gate_out, up_out, down_out = hand_over(
        sizes, gate_weight, up_weight, norm_gain[:, None], down_weight
    )
    experts = gate_out.shape[0]
    floats = tokens.astype(jnp.float32)
    normed = (floats * lax.rsqrt(jnp.mean(floats * floats, axis=1, keepdims=True) + EPS)).astype(
        jnp.bfloat16
    )
    first_share = jax.nn.sigmoid(route_logit[:, 0] - route_logit[:, 1])
    shares = jnp.stack([first_share, 1.0 - first_share], axis=1)
    parts = []
    for e in range(experts):
        weight = jnp.sum(jnp.where(routes == e, shares, 0.0), axis=1, keepdims=True)
        gate_val = jnp.dot(normed, gate_out[e], preferred_element_type=jnp.float32)
        up_val = jnp.dot(normed, up_out[e], preferred_element_type=jnp.float32)
        parts.append((jax.nn.silu(gate_val) * up_val * weight).astype(jnp.bfloat16))
    hidden = jnp.concatenate(parts, axis=1)
    partial = jnp.dot(
        hidden, down_out.reshape(-1, down_out.shape[2]), preferred_element_type=jnp.float32
    )
    mixed = sum_by_axis(partial, FS)
    return (gate_out, up_out, down_out, mixed.astype(jnp.bfloat16))


def solution(mesh):
    sizes = (8, 4, 2, mesh.shape["tp"])
    finer = Mesh(mesh.devices.reshape(sizes), ("fs_0", "fs_1", "fs_2", "tp"))
    in_specs = (
        P("tp", None),
        P(FS),
        P(None, FS, "tp"),
        P(None, FS, "tp"),
        P(None, FS, "tp"),
        P("tp", None),
        P("tp", None),
    )
    out_specs = (P(None, None, FS), P(None, None, FS), P(None, FS, None), P(TP_FS, None))
    return jax.shard_map(
        functools.partial(shards, sizes),
        mesh=finer,
        in_specs=in_specs,
        out_specs=out_specs,
        check_vma=False,
    )
```

time: 329 us -> 232 us (0.71)
  Pallas kernels: 0 us -> 82.3 us
  local copies, waits for them, and re-layouts: 79.5 us -> 13.6 us
  blocking collectives: 66.8 us -> 6.45 us
  waiting for transfers between devices: 132 us -> 95.3 us
  other arithmetic: 16.7 us -> 3.36 us
  starting transfers between devices: 5.86 us -> 1.37 us
    pallas_call x0 -> x1, Pallas kernels: none -> 82.3 us  [hand_over(): pl.pallas_call(functools.partial(weights_kernel, sizes), out_shape=[jax.S...]
    all_to_all x2 -> x0, blocking collectives: 60.3 us -> none  [in_one_piece(): lax.all_to_all(both, axis, split_axis=split_dim, concat_axis=concat_dim,...]
    gather x3 -> x0, local copies, waits for them, and re-layouts: 34.1 us -> none  [the longest x1 12.7 us: shards(): first_rows = jnp.take(flat_rows, flat_slot[:, 0], axis=0)]
    all_to_all x1 -> x0, waiting for transfers between devices: 25.4 us -> none  [copy_for_each(): return lax.all_to_all(copies, axis, split_axis=0, concat_axis=0, tiled=True)]
    all_gather x1 -> x0, waiting for transfers between devices: 11.2 us -> none  [sent_together(): whole = lax.all_gather(both, axis, axis=dim, tiled=True)]
    add x2 -> x0, other arithmetic: 7.32 us -> none  [the longest x1 7.32 us: shards(): shares[:, 0:1] * first_rows + shares[:, 1:2] * second_rows]
    unnamed x19 -> x20, local copies, waits for them, and re-layouts: 15.4 us -> 8.14 us
    concatenate x1 -> x0, local copies, waits for them, and re-layouts: 6.8 us -> none  [in_one_piece(): both = jnp.concatenate(arrays, axis=along)]
  transfers between devices with their start and end apart: 5 -> 3, of which waited for: 5 -> 3; matrix products, arithmetic and copies ran while one was open for 8% -> 0% of each run, Pallas kernels for 0% -> 0%
where the time goes in v1:
time: 232 us; the launch traced here: 231 us
  waiting for transfers between devices  95.3 us (41%)
  Pallas kernels  82.3 us (35%)
  between operations  14.9 us (6%)
  matrix products  13.9 us (6%)
  local copies, waits for them, and re-layouts  13.6 us (6%)
  blocking collectives  6.45 us (3%)
  other arithmetic  3.36 us (1%)
    reduce_scatter x2, waiting for transfers between devices, sum_by_axis(): so_far = lax.psum_scatter(so_far, axis, scatter_dimension=0, tiled=True)  94.8 us
    pallas_call x1, Pallas kernels, hand_over(): pl.pallas_call(functools.partial(weights_kernel, sizes), out_shape=[jax.S...  82.3 us
    unnamed x20, local copies, waits for them, and re-layouts  8.14 us
    unnamed x1, blocking collectives  6.45 us
    dot_general x4, matrix products, shards(): up_val = jnp.dot(normed, up_out[e], preferred_element_type=jnp.float32)  4.71 us
    dot_general x4, matrix products, shards(): gate_val = jnp.dot(normed, gate_out[e], preferred_element_type=jnp.float32)  4.66 us
  transfers between devices with their start and end apart: 3, of which 3 were waited for; matrix products, arithmetic and copies ran while one was open for 0% of the time, Pallas kernels for 0%

profile of v1, /device:TPU:1, one launch (start us, length us, event | category | flops | bytes accessed | tf_op | source)
XLA Modules:
  0.0 231.2 jit_solution(1636788891268967072)
XLA Ops:
  7.2 0.0 reduce-scatter.5.cloned.1.call-start
  7.2 1.3 copy.12.gain_ref
  8.6 0.0 copy-start
  8.6 2.7 %fusion.1 = f32[768]{0:T(1024)S(1)} fusion(bf16[768,2048]{1,0:T(8,128)(2,1)} %param.7), kind=kLoop, calls=%fused_computation.2 | loop fusion | flops 4717824 | bytes 3148800 | tf_op jit(solution)/shard_map/reduce_sum | solution.py:264
  11.3 0.1 copy-done
  11.4 0.0 copy-start.5
  11.4 0.6 fusion.2
  12.0 0.1 copy-done.5
  12.1 82.3 %hand_over.1 = (bf16[4,8,8,32,128]{4,3,2,1,0:T(8,128)(2,1)}, bf16[4,8,8,32,128]{4,3,2,1,0:T(8,128)(2,1)}, bf16[4,128,2048]{2,1,0:T(8,128)(2,1)}) custom-call(f32[4,32,2048]{2,1,0:T(8,128)} %gate_ref.1, f32[4,32,2048]{2,1,0:T(8,128)} %up_ref.1, f32[32,1]{1,0:T(8,128)} %copy.12.gain_ref, f32[4,128,512]{2,1,0:T(8,128)} %down_ref.1), custom_call_target="tpu_custom_call" | custom-call | tf_op jit(solution)/shard_map/hand_over/pallas_call | solution.py:219
  94.5 3.5 %fusion.24 = (bf16[1,8,8,32,128]{4,3,2,1,0:T(8,128)(2,1)S(1)}, bf16[1,8,8,32,128]{4,3,2,1,0:T(8,128)(2,1)S(1)}, bf16[1,8,8,32,128]{4,3,2,1,0:T(8,128)(2,1)S(1)},...) fusion(bf16[4,8,8,32,128]{4,3,2,1,0:T(8,128)(2,1)} %get-tuple-e, ...), kind=kLoop, calls=%fused_computation.38 | loop fusion | bytes 8388608 | tf_op jit(solution)/shard_map/slice | solution.py:272
  98.0 1.2 fusion.26
  99.1 1.2 fusion.27
  100.3 0.0 copy-start.4
  100.3 1.2 fusion.28
  101.5 1.2 fusion.29
  102.7 0.0 copy-done.4
  102.7 1.2 fusion.7
  103.9 1.2 fusion.8
  105.1 1.2 fusion.9
  106.3 0.0 copy-start.1
  106.3 1.2 fusion.10
  107.5 0.4 copy-done.1
  107.9 4.5 %fusion.11 = f32[768,2048]{1,0:T(8,128)} fusion(bf16[512,2048]{1,0:T(8,128)(2,1)S(1)} %bitcast.32, bf16[768,128]{0,1:T(8,128)(2,1)S(1)} %fusion.10, bf16[768,128]{0,1:T(8,128)(2,1)S(1)} %fusion.9, bf16[768,128]{0,1:T(8,128)(2,1)S(1)} %fusion.8, bf16[768,128]{0,1:T(8,128)(2,1)S(1)} %fusion.7), kind=kOutput, calls=%fused_computation.16 | convolution fusion | flops 1613758464 | bytes 9175040 | tf_op jit(solution)/shard_map/dot_general | solution.py:276
  112.4 0.0 copy-start.6
  112.4 0.0 reduce-scatter.5.cloned.1.call-update
  112.4 0.0 copy-start.3
  112.4 0.0 reduce-scatter.7.cloned.1.call-start
  112.5 70.5 %reduce-scatter.5.cloned.1.call-done = f32[96,2048]{1,0:T(8,128)} async-done(((f32[768,2048]{1,0:T(8,128)}), f32[96,2048]{1,0:T(8,128)}) %reduce-scatter.5.cloned.1.call-update) | async-done | bytes 786448 | tf_op jit(solution)/shard_map/reduce_scatter | solution.py:254
  182.9 0.0 reduce-scatter.7.cloned.1.call-update
  182.9 24.3 %reduce-scatter.7.cloned.1.call-done = f32[24,2048]{1,0:T(8,128)} async-done(((f32[96,2048]{1,0:T(8,128)}), f32[24,2048]{1,0:T(8,128)}) %reduce-scatter.7.cloned.1.call-update) | async-done | bytes 196624 | tf_op jit(solution)/shard_map/reduce_scatter | solution.py:254
  207.2 6.5 %fusion = f32[16,2048]{1,0:T(8,128)S(1)} fusion(f32[24,2048]{1,0:T(8,128)} %reduce-scatter.7.cloned.1.call-done), kind=kCustom, calls=%all-reduce-scatter | all-reduce-scatter fusion | flops 65537 | bytes 328704
  213.7 1.3 collective-permute-start
  215.0 0.0 copy-done.6
  215.0 0.6 dynamic-slice.4
  216.3 0.5 collective-permute-done
  216.8 0.2 concatenate.4
  217.0 0.7 dynamic-slice_convert_fusion
  217.7 3.0 %copy.16 = bf16[4,2048,128]{2,1,0:T(8,128)(2,1)} copy(bf16[4,2048,128]{2,1,0:T(8,128)(2,1)} %bitcast.34) | data formatting | bytes 4194304
  220.7 0.0 copy-done.3
  220.7 0.0 copy-start.2
  220.7 1.3 copy.17
  222.0 1.0 copy-done.2
  223.1 1.3 copy.18
  (4 shorter events, 0.1 us)
Async XLA Ops:
  7.2 175.8 %reduce-scatter.5.cloned.1.call-start = ((), (), s32[]{:S(2)}) async-start(), calls=%async_computation.2 | async-start | bytes 7077888 | tf_op jit(solution)/shard_map/reduce_scatter | solution.py:254
  8.6 2.8 %copy-start = (bf16[768,2048]{1,0:T(8,128)(2,1)S(1)}, bf16[768,2048]{1,0:T(8,128)(2,1)}, u32[]{:S(2)}) copy-start(bf16[768,2048]{1,0:T(8,128)(2,1)} %param.7) | copy-start | bytes 9437188
  11.4 0.7 copy-start.5
  100.3 2.4 %copy-start.4 = (s32[768,2]{0,1:T(2,128)S(1)}, s32[768,2]{0,1:T(2,128)}, u32[]{:S(2)}) copy-start(s32[768,2]{0,1:T(2,128)} %param.12) | copy-start | bytes 18436
  106.3 1.6 copy-start.1
  112.4 102.6 %copy-start.6 = (u32[256]{0:T(256)S(1)}, u32[256]{0:T(256)}, u32[]{:S(2)}) copy-start(u32[256]{0:T(256)} %constant.27) | copy-start | bytes 3076
  112.4 108.3 %copy-start.3 = (bf16[4,8,8,32,128]{4,3,2,1,0:T(8,128)(2,1)S(1)}, bf16[4,8,8,32,128]{4,3,2,1,0:T(8,128)(2,1)}, u32[]{:S(2)}) copy-start(bf16[4,8,8,32,128]{4,3,2,1,0:T(8,128)(2,1)} %get-tuple-element.8) | copy-start | bytes 6291460
  112.4 94.8 %reduce-scatter.7.cloned.1.call-start = ((), (), s32[]{:S(2)}) async-start(), calls=%async_computation.3 | async-start | bytes 983040 | tf_op jit(solution)/shard_map/reduce_scatter | solution.py:254
  213.7 3.1 %collective-permute-start = (bf16[4,2048]{1,0:T(4,128)(2,1)S(1)}, bf16[4,2048]{1,0:T(4,128)(2,1)S(1)}, u32[]{:S(2)}, u32[]{:S(2)}) collective-permute-start(bf16[4,2048]{1,0:T(4,128)(2,1)S(1)} %slice.48), channel_id=1, source_target_pairs={{0,4},{1,5},{2,6},{3,7},{8,12},{9,13},{10,14},{11,15},{16,20},{17,... | collective-permute-start | bytes 49160
  220.7 2.3 %copy-start.2 = (bf16[4,128,2048]{2,1,0:T(8,128)(2,1)S(1)}, bf16[4,128,2048]{2,1,0:T(8,128)(2,1)}, u32[]{:S(2)}) copy-start(bf16[4,128,2048]{2,1,0:T(8,128)(2,1)} %get-tuple-element.34) | copy-start | bytes 6291460
Sparse Core Ops, SparseCore 0:
  112.5 70.3 reduce-scatter.4
  185.5 21.7 reduce-scatter.6

commit v2 on v1

--- a/solution.py
+++ b/solution.py
@@ -12,6 +12,8 @@
 TP_FS = ("tp", "fs_0", "fs_1", "fs_2")
 EPS = 0.5
 MESH = pl.DeviceIdType.MESH
+MIB = 1024 * 1024
+VMEM_ONE, VMEM_TWO, VMEM_THREE = 32 * MIB, 40 * MIB, 32 * MIB
 
 
 def weights_kernel(
@@ -20,9 +22,14 @@
     up_ref,
     gain_ref,
     down_ref,
+    token_ref,
+    route_ref,
+    logit_ref,
     gate_out,
     up_out,
     down_out,
+    normed_out,
+    share_out,
     staged,
     spread,
     by_z,
@@ -146,6 +153,24 @@
 
     down_near = ring(2, down_block)
 
+    step = 48
+    def norm_rows(i, carry):
+        at_rows = pl.ds(pl.multiple_of(i * step, step), step)
+        floats = token_ref[at_rows, :].astype(jnp.float32)
+        scale = lax.rsqrt(jnp.mean(floats * floats, axis=1, keepdims=True) + EPS)
+        normed_out[at_rows, :] = (floats * scale).astype(jnp.bfloat16)
+        return carry
+
+    lax.fori_loop(0, token_ref.shape[0] // step, norm_rows, 0)
+    first = 1.0 / (1.0 + jnp.exp(logit_ref[1:2, :] - logit_ref[0:1, :]))
+    lines = [
+        jnp.where(route_ref[0:1, :] == e, first, 0.0)
+        + jnp.where(route_ref[1:2, :] == e, 1.0 - first, 0.0)
+        for e in range(nx)
+    ]
+    lines.append(jnp.zeros((128 - nx, first.shape[1]), jnp.float32))
+    share_out[...] = jnp.concatenate(lines, axis=0).T
+
     z_copies = {}
     for m in (0, 1):
         for d in range(1, nx):
@@ -204,7 +229,7 @@
         copy.wait_send()
 
 
-def hand_over(sizes, gate_weight, up_weight, gain, down_weight):
+def hand_over(sizes, gate_weight, up_weight, gain, down_weight, tokens, routes, logits):
     nz, ny, nc, nx = sizes
     nyc = ny * nc
     nk = nz * nyc
@@ -216,15 +241,17 @@
     steps = nyc - 1
     dma = pltpu.SemaphoreType.DMA
     vmem = pl.BlockSpec(memory_space=pltpu.VMEM)
-    gate, up, down = pl.pallas_call(
+    gate, up, down, normed, share = pl.pallas_call(
         functools.partial(weights_kernel, sizes),
         out_shape=[
             jax.ShapeDtypeStruct((experts, nz, nyc, rows, width), bf),
             jax.ShapeDtypeStruct((experts, nz, nyc, rows, width), bf),
             jax.ShapeDtypeStruct((experts, hid, dcols * nx), bf),
+            jax.ShapeDtypeStruct(tokens.shape, bf),
+            jax.ShapeDtypeStruct((tokens.shape[0], 128), jnp.float32),
         ],
-        in_specs=[vmem] * 4,
-        out_specs=[vmem] * 3,
+        in_specs=[vmem] * 7,
+        out_specs=[vmem] * 5,
         scratch_shapes=[
             pltpu.VMEM((2, nx, per_x, rows, width), bf),
             pltpu.VMEM((2, nk, rows, width), bf),
@@ -241,43 +268,254 @@
             dma((3, 2)),
         ],
         compiler_params=pltpu.CompilerParams(
-            collective_id=0, has_side_effects=True, vmem_limit_bytes=60 * 1024 * 1024
+            collective_id=0, has_side_effects=True, vmem_limit_bytes=VMEM_ONE
         ),
         name="hand_over",
-    )(gate_weight, up_weight, gain, down_weight)
+    )(gate_weight, up_weight, gain, down_weight, tokens, routes, logits)
     full = (experts, nk * rows, width)
-    return gate.reshape(full), up.reshape(full), down
-
-
-def sum_by_axis(so_far, axes):
-    for axis in axes:
-        so_far = lax.psum_scatter(so_far, axis, scatter_dimension=0, tiled=True)
-    return so_far
+    return gate.reshape(full), up.reshape(full), down, normed, share
+
+
+def compute_kernel(
+    sizes, wy, gate_ref, up_ref, down_ref, x_ref, share_ref, gate_out, up_out, down_out, pz, py, sems
+):
+    nz, ny, nc, nx = sizes
+    pairs = ((gate_ref, gate_out), (up_ref, up_out), (down_ref, down_out))
+    copies = [pltpu.make_async_copy(a, b, sems.at[i]) for i, (a, b) in enumerate(pairs)]
+    for copy in copies:
+        copy.start()
+    experts, hid, width = down_ref.shape
+    half = width // nc
+    tiles = 2 if nz % 2 == 0 else 1
+    z_per = nz // tiles
+    rows = x_ref.shape[0] // tiles
+    r = x_ref.shape[0] // (nz * ny)
+
+    def tile(t, carry):
+        at_rows = pl.ds(pl.multiple_of(t * rows, rows), rows)
+        x = x_ref[at_rows, :]
+        parts = []
+        for e in range(experts):
+            both = jnp.concatenate([gate_ref[e], up_ref[e]], axis=1)
+            val = jnp.dot(x, both, preferred_element_type=jnp.float32)
+            gate_val, up_val = val[:, :hid], val[:, hid:]
+            weight = share_ref[at_rows, e : e + 1]
+            hidden = gate_val / (1.0 + jnp.exp(-gate_val)) * up_val
+            parts.append(jnp.where(weight > 0.0, hidden * weight, 0.0).astype(jnp.bfloat16))
+        hidden = jnp.concatenate(parts, axis=1)
+        down = down_ref[...].reshape(experts * hid, width)
+        for c in range(nc):
+            lo = c * half
+            val = jnp.dot(hidden, down[:, lo : lo + wy], preferred_element_type=jnp.float32)
+            val = val.reshape(z_per, ny, r, wy).astype(jnp.bfloat16)
+            for y in range(ny):
+                py[c, y, pl.ds(t * z_per, z_per)] = val[:, y]
+            val = jnp.dot(hidden, down[:, lo + wy : lo + half], preferred_element_type=jnp.float32)
+            pz[c, pl.ds(t * z_per, z_per)] = val.reshape(z_per, ny, r, half - wy).astype(jnp.bfloat16)
+        return carry
+
+    lax.fori_loop(0, tiles, tile, 0)
+    for copy in copies:
+        copy.wait()
+
+
+def compute(sizes, wy, gate, up, down, normed, share):
+    nz, ny, nc, nx = sizes
+    bf = jnp.bfloat16
+    vmem = pl.BlockSpec(memory_space=pltpu.VMEM)
+    hbm = pl.BlockSpec(memory_space=pl.ANY)
+    r = normed.shape[0] // (nz * ny)
+    half = down.shape[2] // nc
+    return pl.pallas_call(
+        functools.partial(compute_kernel, sizes, wy),
+        out_shape=[
+            jax.ShapeDtypeStruct(gate.shape, bf),
+            jax.ShapeDtypeStruct(up.shape, bf),
+            jax.ShapeDtypeStruct(down.shape, bf),
+            jax.ShapeDtypeStruct((nc, nz, ny, r, half - wy), bf),
+            jax.ShapeDtypeStruct((nc, ny, nz, r, wy), bf),
+        ],
+        in_specs=[vmem] * 5,
+        out_specs=[hbm] * 3 + [vmem] * 2,
+        scratch_shapes=[pltpu.SemaphoreType.DMA((3,))],
+        compiler_params=pltpu.CompilerParams(vmem_limit_bytes=VMEM_TWO),
+        name="experts",
+    )(gate, up, down, normed, share)
+
+
+def reduce_kernel(
+    sizes,
+    pz,
+    py,
+    out,
+    cz,
+    cy,
+    sz,
+    sy,
+    rz,
+    ry,
+    tz,
+    ty,
+    qz,
+    qy,
+    whole,
+    other,
+    last,
+    c_send,
+    c_recv,
+    z_send,
+    z_recv,
+    y_send,
+    y_recv,
+):
+    nz, ny, nc, nx = sizes
+    my_z, my_y = lax.axis_index("fs_0"), lax.axis_index("fs_1")
+    my_c, my_x = lax.axis_index("fs_2"), lax.axis_index("tp")
+    f32, bf = jnp.float32, jnp.bfloat16
+
+    def at(dz=0, dy=0, dc=0):
+        return (
+            lax.rem(my_z + dz, nz),
+            lax.rem(my_y + dy, ny),
+            lax.rem(my_c + dc, nc),
+            my_x,
+        )
+
+    twin = at(dc=1)
+    z_peers = [at(dz=d) for d in range(nz)]
+    y_peers = [at(dy=d) for d in range(ny)]
+    peers = [twin] + z_peers[1:] + y_peers[1:]
+    barrier = pltpu.get_barrier_semaphore()
+    for peer in peers:
+        pl.semaphore_signal(barrier, inc=1, device_id=peer, device_id_type=MESH)
+    pl.semaphore_wait(barrier, len(peers))
+
+    sent = []
+
+    def start(src, dst, ssem, rsem, peer):
+        copy = pltpu.make_async_remote_copy(
+            src_ref=src, dst_ref=dst, send_sem=ssem, recv_sem=rsem, device_id=peer, device_id_type=MESH
+        )
+        copy.start()
+        sent.append(copy)
+        return copy
+
+    twin_c = twin[2]
+    c_z = start(pz.at[twin_c], cz, c_send.at[0], c_recv.at[0], twin)
+    c_y = start(py.at[twin_c], cy, c_send.at[1], c_recv.at[1], twin)
+    c_z.wait_recv()
+    z1 = []
+    for d in range(1, nz):
+        z = z_peers[d][0]
+        sz[z] = (pz[my_c, z].astype(f32) + cz[z].astype(f32)).astype(bf)
+        z1.append(start(sz.at[z], rz.at[d], z_send.at[0, d], z_recv.at[0, d], z_peers[d]))
+    c_y.wait_recv()
+    y1 = []
+    for d in range(1, ny):
+        y = y_peers[d][1]
+        for z in range(nz):
+            sy[y, z] = (py[my_c, y, z].astype(f32) + cy[y, z].astype(f32)).astype(bf)
+        y1.append(start(sy.at[y], ry.at[d], y_send.at[0, d], y_recv.at[0, d], y_peers[d]))
+    for copy in y1:
+        copy.wait_recv()
+
+    def sum_y(z):
+        total = py[my_c, my_y, z].astype(f32) + cy[my_y, z].astype(f32)
+        for d in range(1, ny):
+            total = total + ry[d, z].astype(f32)
+        return total
+
+    y2 = []
+    for d in range(1, nz):
+        z = z_peers[d][0]
+        ty[z] = sum_y(z).astype(bf)
+        y2.append(start(ty.at[z], qy.at[d], z_send.at[1, d], z_recv.at[1, d], z_peers[d]))
+    for copy in z1:
+        copy.wait_recv()
+
+    def sum_z(y):
+        total = pz[my_c, my_z, y].astype(f32) + cz[my_z, y].astype(f32)
+        for d in range(1, nz):
+            total = total + rz[d, y].astype(f32)
+        return total
+
+    z2 = []
+    for d in range(1, ny):
+        y = y_peers[d][1]
+        tz[y] = sum_z(y).astype(bf)
+        z2.append(start(tz.at[y], qz.at[d], y_send.at[1, d], y_recv.at[1, d], y_peers[d]))
+    sum_of_z = sum_z(my_y)
+    sum_of_y = sum_y(my_z)
+    for d, copy in zip(range(1, ny), z2):
+        copy.wait_recv()
+        sum_of_z = sum_of_z + qz[d].astype(f32)
+    for d, copy in zip(range(1, nz), y2):
+        copy.wait_recv()
+        sum_of_y = sum_of_y + qy[d].astype(f32)
+    whole[...] = jnp.concatenate([sum_of_y, sum_of_z], axis=1)
+    own = out.shape[0]
+    low, high = whole[0:own, :], whole[own : 2 * own, :]
+    first_core = my_c == 0
+    other[...] = jnp.where(first_core, high, low)
+    swap = start(other, last, c_send.at[2], c_recv.at[2], twin)
+    mine = jnp.where(first_core, low, high)
+    swap.wait_recv()
+    theirs = last[...]
+    left = jnp.where(first_core, mine, theirs)
+    right = jnp.where(first_core, theirs, mine)
+    out[...] = jnp.concatenate([left, right], axis=1).astype(out.dtype)
+    for copy in sent:
+        copy.wait_send()
+
+
+def reduce_scatter(sizes, pz, py):
+    nz, ny, nc, nx = sizes
+    r, wz = pz.shape[3:]
+    wy = py.shape[4]
+    own, half = r // nc, wy + wz
+    bf, f32 = jnp.bfloat16, jnp.float32
+    dma = pltpu.SemaphoreType.DMA
+    vmem = pl.BlockSpec(memory_space=pltpu.VMEM)
+    return pl.pallas_call(
+        functools.partial(reduce_kernel, sizes),
+        out_shape=jax.ShapeDtypeStruct((own, half * nc), bf),
+        in_specs=[vmem] * 2,
+        out_specs=vmem,
+        scratch_shapes=[
+            pltpu.VMEM((nz, ny, r, wz), bf),
+            pltpu.VMEM((ny, nz, r, wy), bf),
+            pltpu.VMEM((nz, ny, r, wz), bf),
+            pltpu.VMEM((ny, nz, r, wy), bf),
+            pltpu.VMEM((nz, ny, r, wz), bf),
+            pltpu.VMEM((ny, nz, r, wy), bf),
+            pltpu.VMEM((ny, r, wz), bf),
+            pltpu.VMEM((nz, r, wy), bf),
+            pltpu.VMEM((ny, r, wz), bf),
+            pltpu.VMEM((nz, r, wy), bf),
+            pltpu.VMEM((r, half), f32),
+            pltpu.VMEM((own, half), f32),
+            pltpu.VMEM((own, half), f32),
+            dma((3,)),
+            dma((3,)),
+            dma((2, nz)),
+            dma((2, nz)),
+            dma((2, ny)),
+            dma((2, ny)),
+        ],
+        compiler_params=pltpu.CompilerParams(
+            collective_id=1, has_side_effects=True, vmem_limit_bytes=VMEM_THREE
+        ),
+        name="sum_up",
+    )(pz, py)
 
 
 def shards(sizes, tokens, norm_gain, gate_weight, up_weight, down_weight, routes, route_logit):
-    gate_out, up_out, down_out = hand_over(
-        sizes, gate_weight, up_weight, norm_gain[:, None], down_weight
+    gate, up, down, normed, share = hand_over(
+        sizes, gate_weight, up_weight, norm_gain[:, None], down_weight, tokens, routes.T, route_logit.T
     )
-    experts = gate_out.shape[0]
-    floats = tokens.astype(jnp.float32)
-    normed = (floats * lax.rsqrt(jnp.mean(floats * floats, axis=1, keepdims=True) + EPS)).astype(
-        jnp.bfloat16
-    )
-    first_share = jax.nn.sigmoid(route_logit[:, 0] - route_logit[:, 1])
-    shares = jnp.stack([first_share, 1.0 - first_share], axis=1)
-    parts = []
-    for e in range(experts):
-        weight = jnp.sum(jnp.where(routes == e, shares, 0.0), axis=1, keepdims=True)
-        gate_val = jnp.dot(normed, gate_out[e], preferred_element_type=jnp.float32)
-        up_val = jnp.dot(normed, up_out[e], preferred_element_type=jnp.float32)
-        parts.append((jax.nn.silu(gate_val) * up_val * weight).astype(jnp.bfloat16))
-    hidden = jnp.concatenate(parts, axis=1)
-    partial = jnp.dot(
-        hidden, down_out.reshape(-1, down_out.shape[2]), preferred_element_type=jnp.float32
-    )
-    mixed = sum_by_axis(partial, FS)
-    return (gate_out, up_out, down_out, mixed.astype(jnp.bfloat16))
+    wy = tokens.shape[1] // sizes[2] * 5 // 8
+    gate_out, up_out, down_out, pz, py = compute(sizes, wy, gate, up, down, normed, share)
+    return (gate_out, up_out, down_out, reduce_scatter(sizes, pz, py))
 
 
 def solution(mesh):

time: 232 us -> 123 us (0.53)
  waiting for transfers between devices: 95.3 us -> 0 us
  Pallas kernels: 82.3 us -> 113 us
  between operations: 14.9 us -> 0.66 us
  matrix products: 13.9 us -> 0 us
  blocking collectives: 6.45 us -> 0 us
  local copies, waits for them, and re-layouts: 13.6 us -> 8.31 us
  other arithmetic: 3.36 us -> 0 us
    reduce_scatter x2 -> x0, waiting for transfers between devices: 94.8 us -> none  [sum_by_axis(): so_far = lax.psum_scatter(so_far, axis, scatter_dimension=0, tiled=True)]
    pallas_call x0 -> x2, Pallas kernels: none -> 35.8 us  [the longest x1 30.1 us: reduce_scatter(): pl.pallas_call(functools.partial(reduce_kernel, sizes), out_shape=jax.Sha...]
    dot_general x9 -> x0, matrix products: 13.9 us -> none  [the longest x4 4.71 us: shards(): up_val = jnp.dot(normed, up_out[e], preferred_element_type=jnp.float32)]
    unnamed x1 -> x0, blocking collectives: 6.45 us -> none
    pallas_call x1, Pallas kernels: 82.3 us -> 77.7 us  [hand_over(): pl.pallas_call(functools.partial(weights_kernel, sizes), out_shape=[jax.S...]
    slice x1 -> x0, local copies, waits for them, and re-layouts: 3.5 us -> none  [shards(): gate_val = jnp.dot(normed, gate_out[e], preferred_element_type=jnp.float32)]
    reduce_sum x2 -> x0, other arithmetic: 2.76 us -> none  [the longest x1 2.72 us: shards(): jnp.mean(floats * floats, axis=1, keepdims=True) + EPS]
    unnamed x20 -> x13, local copies, waits for them, and re-layouts: 8.14 us -> 7.58 us
  transfers between devices with their start and end apart: 3 -> 0, of which waited for: 3 -> 0; matrix products, arithmetic and copies ran while one was open for 0% -> 0% of each run, Pallas kernels for 0% -> 0%
where the time goes in v2:
time: 123 us; the launch traced here: 122 us
  Pallas kernels  113 us (92%)
  local copies, waits for them, and re-layouts  8.31 us (7%)
    pallas_call x1, Pallas kernels, hand_over(): pl.pallas_call(functools.partial(weights_kernel, sizes), out_shape=[jax.S...  77.7 us
    pallas_call x1, Pallas kernels, reduce_scatter(): pl.pallas_call(functools.partial(reduce_kernel, sizes), out_shape=jax.Sha...  30.1 us
    unnamed x13, local copies, waits for them, and re-layouts  7.58 us
    pallas_call x1, Pallas kernels, compute(): pl.pallas_call(functools.partial(compute_kernel, sizes, wy), out_shape=[j...  5.73 us

profile of v2, /device:TPU:1, one launch (start us, length us, event | category | flops | bytes accessed | tf_op | source)
XLA Modules:
  0.0 122.4 jit_solution(16864404228402909670)
XLA Ops:
  0.6 0.7 copy.11.gain_ref
  1.4 0.0 copy-start
  1.4 1.9 %copy-done = bf16[768,2048]{1,0:T(8,128)(2,1)S(1)} copy-done((bf16[768,2048]{1,0:T(8,128)(2,1)S(1)}, bf16[768,2048]{1,0:T(8,128)(2,1)}, u32[]{:S(2)}) %copy-start) | copy-done | bytes 3145752
  3.3 0.0 copy-start.1
  3.3 1.2 copy-done.1
  4.5 0.0 copy-start.2
  4.5 1.2 copy-done.2
  5.7 0.0 copy-start.3
  5.7 1.2 copy-done.3
  6.9 0.0 copy-start.4
  6.9 0.7 copy-done.4
  7.6 0.0 copy-start.5
  7.6 0.7 copy-done.5
  8.3 77.7 %hand_over.1 = (bf16[4,8,8,32,128]{4,3,2,1,0:T(8,128)(2,1)S(1)}, bf16[4,8,8,32,128]{4,3,2,1,0:T(8,128)(2,1)S(1)}, bf16[4,128,2048]{2,1,0:T(8,128)(2,1)S(1)}, bf16[768,2048]{1,0:T(8,128)(2,1)S(1)}, f32[768,128]{1,0:T(8,128)S(1)}) custom-call(f32[4,32,2048]{2,1,0:T(8,128)S(1)} %copy-done.1, f32[4,32,2048]{2,1,0:T(8,128)S(1)} %copy-done.2, ...), custom_call_target="tpu_custom_call" | custom-call | tf_op jit(solution)/shard_map/hand_over/pallas_call | solution.py:244
  86.0 5.7 %experts.1 = (bf16[4,2048,128]{2,1,0:T(8,128)(2,1)}, bf16[4,2048,128]{2,1,0:T(8,128)(2,1)}, bf16[4,128,2048]{2,1,0:T(8,128)(2,1)}, bf16[2,8,4,24,384]{4,3,2,1,0:...) custom-call(bf16[4,2048,128]{2,1,0:T(8,128)(2,1)S(1)} %bitcast.5, bf16[4,2048,128]{2,1,0:T(8,128)(2,1)S(1)} %bitcast.6, ...), custom_call_target="tpu_custom_call" | custom-call | tf_op jit(solution)/shard_map/experts/pallas_call | solution.py:329
  91.7 30.1 %sum_up.1 = bf16[12,2048]{1,0:T(8,128)(2,1)S(1)} custom-call(bf16[2,8,4,24,384]{4,3,2,1,0:T(8,128)(2,1)S(1)} %get-tuple-element.22.pz, bf16[2,4,8,24,640]{4,3,2,1,0:T(8,128)(2,1)S(1)} %get-tuple-element.23.py), custom_call_target="tpu_custom_call" | custom-call | tf_op jit(solution)/shard_map/sum_up/pallas_call | solution.py:479
  121.8 0.6 copy.13
Async XLA Ops:
  1.4 1.9 %copy-start = (bf16[768,2048]{1,0:T(8,128)(2,1)S(1)}, bf16[768,2048]{1,0:T(8,128)(2,1)}, u32[]{:S(2)}) copy-start(bf16[768,2048]{1,0:T(8,128)(2,1)} %token_ref.1) | copy-start | bytes 9437188
  3.3 1.2 %copy-start.1 = (f32[4,32,2048]{2,1,0:T(8,128)S(1)}, f32[4,32,2048]{2,1,0:T(8,128)}, u32[]{:S(2)}) copy-start(f32[4,32,2048]{2,1,0:T(8,128)} %gate_ref.1) | copy-start | bytes 3145732
  4.5 1.2 %copy-start.2 = (f32[4,32,2048]{2,1,0:T(8,128)S(1)}, f32[4,32,2048]{2,1,0:T(8,128)}, u32[]{:S(2)}) copy-start(f32[4,32,2048]{2,1,0:T(8,128)} %up_ref.1) | copy-start | bytes 3145732
  5.7 1.2 %copy-start.3 = (f32[4,128,512]{2,1,0:T(8,128)S(1)}, f32[4,128,512]{2,1,0:T(8,128)}, u32[]{:S(2)}) copy-start(f32[4,128,512]{2,1,0:T(8,128)} %down_ref.1) | copy-start | bytes 3145732
  6.9 0.7 copy-start.4
  7.6 0.7 copy-start.5

commit v3 on v1

v3 whole, which is shorter than its diff:
```python
import functools

import jax
import jax.numpy as jnp
from jax import lax
from jax.experimental import pallas as pl
from jax.experimental.pallas import tpu as pltpu
from jax.sharding import Mesh
from jax.sharding import PartitionSpec as P

FS = ("fs_0", "fs_1", "fs_2")
TP_FS = ("tp", "fs_0", "fs_1", "fs_2")
EPS = 0.5
MESH = pl.DeviceIdType.MESH
MIB = 1024 * 1024
PARTS = 2


def whole_kernel(
    sizes,
    gate_hbm,
    up_hbm,
    gain_ref,
    down_hbm,
    token_hbm,
    route_ref,
    logit_ref,
    gate_out,
    up_out,
    down_out,
    mixed_out,
    gate_in,
    up_in,
    down_in,
    token_in,
    staged,
    spread,
    by_z,
    normed,
    share,
    hidden,
    part,
    from_twin,
    to_y,
    from_y,
    to_z,
    from_z,
    total,
    other,
    last,
    in_sem,
    a_send,
    a_recv,
    z_send,
    z_recv,
    y_send,
    y_recv,
    c_send,
    c_recv,
    f_send,
    f_recv,
    t_send,
    t_recv,
    ry_send,
    ry_recv,
    rz_send,
    rz_recv,
):
    nz, ny, nc, nx = sizes
    nyc = ny * nc
    nk = nz * nyc
    per_x = nk // nx
    f32, bf = jnp.float32, jnp.bfloat16
    my_z, my_y = lax.axis_index("fs_0"), lax.axis_index("fs_1")
    my_c, my_x = lax.axis_index("fs_2"), lax.axis_index("tp")
    my_yc = my_y * nc + my_c
    outs = (gate_out, up_out)

    loads = [
        pltpu.make_async_copy(src, dst, in_sem.at[i])
        for i, (src, dst) in enumerate(
            ((gate_hbm, gate_in), (up_hbm, up_in), (down_hbm, down_in), (token_hbm, token_in))
        )
    ]
    for load in loads:
        load.start()

    def at(dz=0, dy=0, dc=0, dx=0):
        return (
            lax.rem(my_z + dz, nz),
            lax.rem(my_y + dy, ny),
            lax.rem(my_c + dc, nc),
            lax.rem(my_x + dx, nx),
        )

    yc_steps = [(dy, dc) for dy in range(ny) for dc in range(nc) if dy + dc > 0]
    peers = (
        [at(dx=d) for d in range(1, nx)]
        + [at(dz=d) for d in range(1, nz)]
        + [at(dy=dy, dc=dc) for dy, dc in yc_steps]
    )
    barrier = pltpu.get_barrier_semaphore()
    for peer in peers:
        pl.semaphore_signal(barrier, inc=1, device_id=peer, device_id_type=MESH)

    sent = []

    def start(src, dst, ssem, rsem, peer):
        copy = pltpu.make_async_remote_copy(
            src_ref=src, dst_ref=dst, send_sem=ssem, recv_sem=rsem, device_id=peer, device_id_type=MESH
        )
        copy.start()
        sent.append(copy)
        return copy

    rows = gate_in.shape[1]
    width = gate_in.shape[2] // per_x
    sub = rows // PARTS
    gain_row = gain_ref[...]
    same = lax.broadcasted_iota(jnp.int32, (rows, rows), 0) == lax.broadcasted_iota(
        jnp.int32, (rows, rows), 1
    )
    gain = jnp.sum(jnp.where(same, gain_row, 0.0), axis=1, keepdims=True)
    chunks = [(m, h) for m in (0, 1) for h in range(PARTS)]

    a_copies = {}
    for m, ref in ((0, gate_in), (1, up_in)):
        loads[m].wait()
        for h in range(PARTS):
            lo = h * sub
            for d in range(nx):
                expert = lax.rem(my_x + d, nx)
                for k in range(per_x):
                    block = ref[expert, lo : lo + sub, k * width : (k + 1) * width]
                    block = (block * gain[lo : lo + sub]).astype(bf)
                    if d == 0:
                        spread[m, h, my_x * per_x + k] = block
                    else:
                        staged[m, h, d, k] = block
            if m + h == 0:
                pl.semaphore_wait(barrier, len(peers))
            for d in range(1, nx):
                a_copies[m, h, d] = start(
                    staged.at[m, h, d],
                    spread.at[m, h, pl.ds(my_x * per_x, per_x)],
                    a_send.at[m, h, d],
                    a_recv.at[m, h, d],
                    at(dx=d),
                )

    cols = down_in.shape[2]
    half_e = nx // 2
    loads[2].wait()
    own_cols = pl.ds(pl.multiple_of(my_x * cols, cols), cols)
    for e in range(nx):
        down_out[e, :, own_cols] = down_in[e].astype(bf)

    left, right = lax.rem(my_x + nx - 1, nx), lax.rem(my_x + 1, nx)

    def near(tag, block, side, h):
        ref = block(my_x, h)
        return start(
            ref, ref, c_send.at[tag, side, h], c_recv.at[tag, side, h], at(dx=1 if side == 0 else nx - 1)
        )

    def pass_on(tag, block, side):
        ref = block(left if side == 0 else right, side)
        return start(
            ref, ref, f_send.at[tag, side], f_recv.at[tag, side], at(dx=1 if side == 0 else nx - 1)
        )

    def down_block(x, h):
        return down_out.at[
            pl.ds(h * half_e, half_e), :, pl.ds(pl.multiple_of(x * cols, cols), cols)
        ]

    d_tag = len(chunks)
    d_near = {(s, s): near(d_tag, down_block, s, s) for s in (0, 1)}

    loads[3].wait()
    step = 48

    def norm_rows(i, carry):
        at_rows = pl.ds(pl.multiple_of(i * step, step), step)
        floats = token_in[at_rows, :].astype(f32)
        scale = lax.rsqrt(jnp.mean(floats * floats, axis=1, keepdims=True) + EPS)
        normed[at_rows, :] = (floats * scale).astype(bf)
        return carry

    lax.fori_loop(0, token_in.shape[0] // step, norm_rows, 0)
    first = 1.0 / (1.0 + jnp.exp(logit_ref[1:2, :] - logit_ref[0:1, :]))
    lines = [
        jnp.where(route_ref[0:1, :] == e, first, 0.0)
        + jnp.where(route_ref[1:2, :] == e, 1.0 - first, 0.0)
        for e in range(nx)
    ]
    lines.append(jnp.zeros((128 - nx, first.shape[1]), f32))
    columns = jnp.concatenate(lines, axis=0).T
    for e in range(nx):
        share[e] = jnp.broadcast_to(columns[:, e : e + 1], share.shape[1:])

    z_copies, y_copies, c_near, c_far = {}, {}, {}, {}
    half_z = nz // 2

    def over_z(q):
        m, h = q
        for d in range(1, nx):
            a_copies[m, h, d].wait_recv()
        for dz in range(1, nz):
            peer = at(dz=dz)
            z_copies[q, dz] = start(
                spread.at[m, h, pl.ds(peer[0] * nyc, nyc)],
                by_z.at[m, h, my_z],
                z_send.at[m, h, dz],
                z_recv.at[m, h, dz],
                peer,
            )
        by_z[m, h, my_z] = spread[m, h, pl.ds(my_z * nyc, nyc)]

    def over_yc(q):
        m, h = q
        out, lo = outs[m], h * sub
        for dz in range(1, nz):
            z_copies[q, dz].wait_recv()
        for i, (dy, dc) in enumerate(yc_steps):
            peer = at(dy=dy, dc=dc)
            y_copies[q, i] = start(
                by_z.at[m, h, :, peer[1] * nc + peer[2]],
                out.at[my_x, :, my_yc, pl.ds(lo, sub)],
                y_send.at[m, h, i],
                y_recv.at[m, h, i],
                peer,
            )
        out[my_x, :, my_yc, lo : lo + sub, :] = by_z[m, h, :, my_yc]

    def out_block(q):
        m, h = q
        return lambda x, half: outs[m].at[x, pl.ds(half * half_z, half_z), :, pl.ds(h * sub, sub)]

    def over_x(q):
        tag = chunks.index(q)
        for i in range(len(yc_steps)):
            y_copies[q, i].wait_recv()
        for s in (0, 1):
            c_near[q, s, s] = near(tag, out_block(q), s, s)
        for s in (0, 1):
            c_near[q, s, 1 - s] = near(tag, out_block(q), s, 1 - s)

    def onward(q):
        for s in (0, 1):
            c_near[q, s, s].wait_recv()
            c_far[q, s] = pass_on(chunks.index(q), out_block(q), s)

    experts = nx
    hid = width
    tiles = 2
    tile_rows = normed.shape[0] // tiles
    z_per = nz // tiles
    r = normed.shape[0] // (nz * ny)

    def run_expert(e):
        def tile(t, carry):
            at_rows = pl.ds(pl.multiple_of(t * tile_rows, tile_rows), tile_rows)
            shape = (nk * rows, width)
            both = jnp.concatenate([gate_out[e].reshape(shape), up_out[e].reshape(shape)], axis=1)
            val = jnp.dot(normed[at_rows, :], both, preferred_element_type=f32)
            gate_val, up_val = val[:, :hid], val[:, hid:]
            weight = share[e, at_rows, :]
            value = gate_val / (1.0 + jnp.exp(-gate_val)) * up_val
            hidden[e, at_rows, :] = jnp.where(weight > 0.0, value * weight, 0.0).astype(bf)
            return carry

        lax.fori_loop(0, tiles, tile, 0)

    q0, q1, q2, q3 = chunks
    over_z(q0)
    over_z(q1)
    over_z(q2)
    over_yc(q0)
    over_z(q3)
    over_x(q0)
    over_yc(q1)
    onward(q0)
    over_x(q1)
    over_yc(q2)
    onward(q1)
    over_x(q2)
    over_yc(q3)
    onward(q2)
    over_x(q3)
    run_expert(my_x)
    onward(q3)
    for s in (0, 1):
        d_near[s, 1 - s] = near(d_tag, down_block, s, 1 - s)
    d_far = []
    for s in (0, 1):
        d_near[s, s].wait_recv()
        d_far.append(pass_on(d_tag, down_block, s))
    for s, e in ((0, left), (1, right)):
        for q in chunks:
            c_near[q, s, 1 - s].wait_recv()
        run_expert(e)
    for q in chunks:
        for s in (0, 1):
            c_far[q, s].wait_recv()
    run_expert(lax.rem(my_x + nx // 2, nx))

    half = cols // nc
    twin = at(dc=1)
    y_peers = [at(dy=d) for d in range(ny)]
    z_peers = [at(dz=d) for d in range(nz)]
    blocks = [my_x, left, right, lax.rem(my_x + nx // 2, nx)]
    twin_copies, sum_y_copies, sum_z_copies = {}, {}, {}

    def multiply(b):
        at_cols = pl.ds(pl.multiple_of(blocks[b] * cols, cols), cols)

        def tile(t, carry):
            at_rows = pl.ds(pl.multiple_of(t * tile_rows, tile_rows), tile_rows)
            units = jnp.concatenate([hidden[e, at_rows, :] for e in range(experts)], axis=1)
            down = down_out[:, :, at_cols].reshape(experts * hid, cols)
            val = jnp.dot(units, down, preferred_element_type=f32)
            val = val.reshape(z_per, ny, r, cols).astype(bf)
            for c in range(nc):
                for y in range(ny):
                    part[b, c, y, pl.ds(t * z_per, z_per)] = val[:, y, :, c * half : (c + 1) * half]
            return carry

        lax.fori_loop(0, tiles, tile, 0)
        twin_copies[b] = start(
            part.at[b, twin[2]], from_twin.at[b], t_send.at[b], t_recv.at[b], twin
        )

    def sum_over_y(b):
        twin_copies[b].wait_recv()
        for d in range(1, ny):
            y = y_peers[d][1]
            to_y[b, y] = (part[b, my_c, y].astype(f32) + from_twin[b, y].astype(f32)).astype(bf)
            sum_y_copies[b, d] = start(
                to_y.at[b, y], from_y.at[b, d], ry_send.at[b, d], ry_recv.at[b, d], y_peers[d]
            )

    def summed(b, z):
        value = part[b, my_c, my_y, z].astype(f32) + from_twin[b, my_y, z].astype(f32)
        for d in range(1, ny):
            value = value + from_y[b, d, z].astype(f32)
        return value

    def sum_over_z(b):
        for d in range(1, ny):
            sum_y_copies[b, d].wait_recv()
        for d in range(1, nz):
            z = z_peers[d][0]
            to_z[b, z] = summed(b, z).astype(bf)
            sum_z_copies[b, d] = start(
                to_z.at[b, z], from_z.at[b, d], rz_send.at[b, d], rz_recv.at[b, d], z_peers[d]
            )

    def finish(b):
        value = summed(b, my_z)
        for d in range(1, nz):
            sum_z_copies[b, d].wait_recv()
            value = value + from_z[b, d].astype(f32)
        total[b] = value

    multiply(0)
    d_near[0, 1].wait_recv()
    multiply(1)
    sum_over_y(0)
    d_near[1, 0].wait_recv()
    multiply(2)
    sum_over_y(1)
    sum_over_z(0)
    sum_over_y(2)
    for copy in d_far:
        copy.wait_recv()
    multiply(3)
    sum_over_z(1)
    sum_over_y(3)
    finish(0)
    sum_over_z(2)
    finish(1)
    sum_over_z(3)
    finish(2)
    finish(3)

    own = mixed_out.shape[0]
    first_core = my_c == 0
    low, high = total[:, 0:own, :], total[:, own : 2 * own, :]
    other[...] = jnp.where(first_core, high, low)
    swap = start(other, last, t_send.at[len(blocks)], t_recv.at[len(blocks)], twin)
    mine = jnp.where(first_core, low, high)
    swap.wait_recv()
    theirs = last[...]
    for b, x in enumerate(blocks):
        pair = [
            jnp.where(first_core, mine[b], theirs[b]),
            jnp.where(first_core, theirs[b], mine[b]),
        ]
        at_cols = pl.ds(pl.multiple_of(x * cols, cols), cols)
        mixed_out[:, at_cols] = jnp.concatenate(pair, axis=1).astype(bf)
    for copy in sent:
        copy.wait_send()


def away(array):
    return pltpu.with_memory_space_constraint(array, pltpu.HBM)


def whole(sizes, gate_weight, up_weight, gain, down_weight, tokens, routes, logits):
    nz, ny, nc, nx = sizes
    nyc = ny * nc
    nk = nz * nyc
    per_x = nk // nx
    experts, rows, cols = gate_weight.shape
    width = cols // per_x
    hid, dcols = down_weight.shape[1:]
    bf, f32 = jnp.bfloat16, jnp.float32
    steps = nyc - 1
    sub = rows // PARTS
    count = tokens.shape[0]
    r = count // (nz * ny)
    half = dcols // nc
    dma = pltpu.SemaphoreType.DMA
    vmem = pl.BlockSpec(memory_space=pltpu.VMEM)
    hbm = pl.BlockSpec(memory_space=pltpu.HBM)
    return pl.pallas_call(
        functools.partial(whole_kernel, sizes),
        out_shape=[
            pltpu.VMEM((experts, nz, nyc, rows, width), bf),
            pltpu.VMEM((experts, nz, nyc, rows, width), bf),
            pltpu.VMEM((experts, hid, dcols * nx), bf),
            pltpu.VMEM((count // nk, dcols * nx), bf),
        ],
        in_specs=[hbm, hbm, vmem, hbm, hbm, vmem, vmem],
        out_specs=[vmem] * 4,
        scratch_shapes=[
            pltpu.VMEM(gate_weight.shape, f32),
            pltpu.VMEM(up_weight.shape, f32),
            pltpu.VMEM(down_weight.shape, f32),
            pltpu.VMEM(tokens.shape, bf),
            pltpu.VMEM((2, PARTS, nx, per_x, sub, width), bf),
            pltpu.VMEM((2, PARTS, nk, sub, width), bf),
            pltpu.VMEM((2, PARTS, nz, nyc, sub, width), bf),
            pltpu.VMEM(tokens.shape, bf),
            pltpu.VMEM((experts, count, hid), f32),
            pltpu.VMEM((experts, count, hid), bf),
            pltpu.VMEM((nx, nc, ny, nz, r, half), bf),
            pltpu.VMEM((nx, ny, nz, r, half), bf),
            pltpu.VMEM((nx, ny, nz, r, half), bf),
            pltpu.VMEM((nx, ny, nz, r, half), bf),
            pltpu.VMEM((nx, nz, r, half), bf),
            pltpu.VMEM((nx, nz, r, half), bf),
            pltpu.VMEM((nx, r, half), f32),
            pltpu.VMEM((nx, r // nc, half), f32),
            pltpu.VMEM((nx, r // nc, half), f32),
            dma((4,)),
            dma((2, PARTS, nx)),
            dma((2, PARTS, nx)),
            dma((2, PARTS, nz)),
            dma((2, PARTS, nz)),
            dma((2, PARTS, steps)),
            dma((2, PARTS, steps)),
            dma((2 * PARTS + 1, 2, 2)),
            dma((2 * PARTS + 1, 2, 2)),
            dma((2 * PARTS + 1, 2)),
            dma((2 * PARTS + 1, 2)),
            dma((nx + 1,)),
            dma((nx + 1,)),
            dma((nx, ny)),
            dma((nx, ny)),
            dma((nx, nz)),
            dma((nx, nz)),
        ],
        compiler_params=pltpu.CompilerParams(
            collective_id=0, has_side_effects=True, vmem_limit_bytes=44 * MIB
        ),
        name="whole",
    )(*(away(a) for a in (gate_weight, up_weight)), gain, away(down_weight), away(tokens), routes, logits)


def write_kernel(a, b, c, a_out, b_out, c_out, sems):
    pairs = ((a, a_out), (b, b_out), (c, c_out))
    copies = [pltpu.make_async_copy(src, dst, sems.at[i]) for i, (src, dst) in enumerate(pairs)]
    for copy in copies:
        copy.start()
    for copy in copies:
        copy.wait()


def write_out(*arrays):
    return pl.pallas_call(
        write_kernel,
        out_shape=[jax.ShapeDtypeStruct(a.shape, a.dtype) for a in arrays],
        in_specs=[pl.BlockSpec(memory_space=pltpu.VMEM)] * len(arrays),
        out_specs=[pl.BlockSpec(memory_space=pltpu.HBM)] * len(arrays),
        scratch_shapes=[pltpu.SemaphoreType.DMA((len(arrays),))],
        compiler_params=pltpu.CompilerParams(vmem_limit_bytes=12 * MIB),
        name="write_out",
    )(*arrays)


def shards(sizes, tokens, norm_gain, gate_weight, up_weight, down_weight, routes, route_logit):
    gate, up, down, mixed = whole(
        sizes, gate_weight, up_weight, norm_gain[None, :], down_weight, tokens, routes.T, route_logit.T
    )
    full = (gate.shape[0], -1, gate.shape[-1])
    gate_out, up_out, down_out = write_out(gate.reshape(full), up.reshape(full), down)
    return (gate_out, up_out, down_out, mixed)


def solution(mesh):
    sizes = (8, 4, 2, mesh.shape["tp"])
    finer = Mesh(mesh.devices.reshape(sizes), ("fs_0", "fs_1", "fs_2", "tp"))
    in_specs = (
        P("tp", None),
        P(FS),
        P(None, FS, "tp"),
        P(None, FS, "tp"),
        P(None, FS, "tp"),
        P("tp", None),
        P("tp", None),
    )
    out_specs = (P(None, None, FS), P(None, None, FS), P(None, FS, None), P(TP_FS, None))
    return jax.shard_map(
        functools.partial(shards, sizes),
        mesh=finer,
        in_specs=in_specs,
        out_specs=out_specs,
        check_vma=False,
    )
```

time: 232 us -> 108 us (0.47)
  waiting for transfers between devices: 95.3 us -> 0 us
  Pallas kernels: 82.3 us -> 105 us
  between operations: 14.9 us -> 0.66 us
  matrix products: 13.9 us -> 0 us
  local copies, waits for them, and re-layouts: 13.6 us -> 2.66 us
  blocking collectives: 6.45 us -> 0 us
  other arithmetic: 3.36 us -> 0 us
    reduce_scatter x2 -> x0, waiting for transfers between devices: 94.8 us -> none  [sum_by_axis(): so_far = lax.psum_scatter(so_far, axis, scatter_dimension=0, tiled=True)]
    pallas_call x1 -> x2, Pallas kernels: 82.3 us -> 105 us  [the longest x1 102 us: whole(): pl.pallas_call(functools.partial(whole_kernel, sizes), out_shape=[pltpu.V...]
    dot_general x9 -> x0, matrix products: 13.9 us -> none  [the longest x4 4.71 us: shards(): up_val = jnp.dot(normed, up_out[e], preferred_element_type=jnp.float32)]
    unnamed x1 -> x0, blocking collectives: 6.45 us -> none
    unnamed x20 -> x7, local copies, waits for them, and re-layouts: 8.14 us -> 2.66 us
    slice x1 -> x0, local copies, waits for them, and re-layouts: 3.5 us -> none  [shards(): gate_val = jnp.dot(normed, gate_out[e], preferred_element_type=jnp.float32)]
    reduce_sum x2 -> x0, other arithmetic: 2.76 us -> none  [the longest x1 2.72 us: shards(): jnp.mean(floats * floats, axis=1, keepdims=True) + EPS]
  transfers between devices with their start and end apart: 3 -> 0, of which waited for: 3 -> 0; matrix products, arithmetic and copies ran while one was open for 0% -> 0% of each run, Pallas kernels for 0% -> 0%
where the time goes in v3:
time: 108 us
  Pallas kernels  105 us (97%)
  local copies, waits for them, and re-layouts  2.66 us (2%)
    pallas_call x1, Pallas kernels, whole(): pl.pallas_call(functools.partial(whole_kernel, sizes), out_shape=[pltpu.V...  102 us
    pallas_call x1, Pallas kernels, write_out(): pl.pallas_call(write_kernel, out_shape=[jax.ShapeDtypeStruct(a.shape, a.d...  2.73 us
    unnamed x7, local copies, waits for them, and re-layouts  2.66 us

profile of v3, /device:TPU:1, one launch (start us, length us, event | category | flops | bytes accessed | tf_op | source)
XLA Modules:
  0.0 108.0 jit_solution(3718369643989076837)
XLA Ops:
  0.6 0.0 copy-start
  0.6 0.7 copy-done
  1.3 0.0 copy-start.1
  1.3 0.7 copy-done.1
  2.0 0.0 copy-start.2
  2.0 0.7 copy-done.2
  2.7 102.0 %whole.1 = (bf16[4,8,8,32,128]{4,3,2,1,0:T(8,128)(2,1)S(1)}, bf16[4,8,8,32,128]{4,3,2,1,0:T(8,128)(2,1)S(1)}, bf16[4,128,2048]{2,1,0:T(8,128)(2,1)S(1)}, bf16[12,2048]{1,0:T(8,128)(2,1)S(1)}) custom-call(f32[4,32,2048]{2,1,0:T(8,128)} %gate_hbm.1, f32[4,32,2048]{2,1,0:T(8,128)} %up_hbm.1, f32[1,32]{1,0:T(1,128)S(1)} %bitcast.9, f32[4,128,512]{2,1,0:T(8,128)} %down_hbm.1, ...), custom_call_target="tpu_custom_call" | custom-call | tf_op jit(solution)/shard_map/whole/pallas_call | solution.py:427
  104.7 2.7 %write_out.1 = (bf16[4,2048,128]{2,1,0:T(8,128)(2,1)}, bf16[4,2048,128]{2,1,0:T(8,128)(2,1)}, bf16[4,128,2048]{2,1,0:T(8,128)(2,1)}) custom-call(bf16[4,2048,128]{2,1,0:T(8,128)(2,1)S(1)} %bitcast.5, bf16[4,2048,128]{2,1,0:T(8,128)(2,1)S(1)} %bitcast.6, bf16[4,128,2048]{2,1,0:T(8,128)(2,1)S(1)} %get-tuple-element.13.c), custom_call_target="tpu_custom_call" | custom-call | tf_op jit(solution)/shard_map/write_out/pallas_call | solution.py:492
  107.4 0.6 copy.12
Async XLA Ops:
  0.6 0.7 copy-start
  1.3 0.7 copy-start.1
  2.0 0.7 copy-start.2

commit v4 on v3

--- a/solution.py
+++ b/solution.py
@@ -13,6 +13,8 @@
 EPS = 0.5
 MESH = pl.DeviceIdType.MESH
 MIB = 1024 * 1024
+SPLIT = 1
+DIRECT = ()
 PARTS = 2
 
 
@@ -20,11 +22,11 @@
     sizes,
     gate_hbm,
     up_hbm,
-    gain_ref,
+    gain_hbm,
     down_hbm,
     token_hbm,
-    route_ref,
-    logit_ref,
+    route_hbm,
+    logit_hbm,
     gate_out,
     up_out,
     down_out,
@@ -33,6 +35,9 @@
     up_in,
     down_in,
     token_in,
+    gain_ref,
+    route_ref,
+    logit_ref,
     staged,
     spread,
     by_z,
@@ -43,6 +48,8 @@
     from_twin,
     to_y,
     from_y,
+    far_in,
+    of_y,
     to_z,
     from_z,
     total,
@@ -79,11 +86,19 @@
     loads = [
         pltpu.make_async_copy(src, dst, in_sem.at[i])
         for i, (src, dst) in enumerate(
-            ((gate_hbm, gate_in), (up_hbm, up_in), (down_hbm, down_in), (token_hbm, token_in))
+            (
+                (gate_hbm, gate_in),
+                (up_hbm, up_in),
+                (down_hbm, down_in),
+                (token_hbm, token_in),
+                (gain_hbm, gain_ref),
+                (route_hbm, route_ref),
+                (logit_hbm, logit_ref),
+            )
         )
     ]
-    for load in loads:
-        load.start()
+    for i in (4, 0, 1, 2, 5, 6, 3):
+        loads[i].start()
 
     def at(dz=0, dy=0, dc=0, dx=0):
         return (
@@ -116,6 +131,7 @@
     rows = gate_in.shape[1]
     width = gate_in.shape[2] // per_x
     sub = rows // PARTS
+    loads[4].wait()
     gain_row = gain_ref[...]
     same = lax.broadcasted_iota(jnp.int32, (rows, rows), 0) == lax.broadcasted_iota(
         jnp.int32, (rows, rows), 1
@@ -175,7 +191,11 @@
         ]
 
     d_tag = len(chunks)
-    d_near = {(s, s): near(d_tag, down_block, s, s) for s in (0, 1)}
+    d_near = {}
+    for s in (0, 1):
+        d_near[s, s] = near(d_tag, down_block, s, s)
+    for s in (0, 1):
+        d_near[s, 1 - s] = near(d_tag, down_block, s, 1 - s)
 
     loads[3].wait()
     step = 48
@@ -188,6 +208,8 @@
         return carry
 
     lax.fori_loop(0, token_in.shape[0] // step, norm_rows, 0)
+    loads[5].wait()
+    loads[6].wait()
     first = 1.0 / (1.0 + jnp.exp(logit_ref[1:2, :] - logit_ref[0:1, :]))
     lines = [
         jnp.where(route_ref[0:1, :] == e, first, 0.0)
@@ -290,8 +312,6 @@
     over_x(q3)
     run_expert(my_x)
     onward(q3)
-    for s in (0, 1):
-        d_near[s, 1 - s] = near(d_tag, down_block, s, 1 - s)
     d_far = []
     for s in (0, 1):
         d_near[s, s].wait_recv()
@@ -305,25 +325,30 @@
             c_far[q, s].wait_recv()
     run_expert(lax.rem(my_x + nx // 2, nx))
 
-    half = cols // nc
+    piece = cols // SPLIT
+    half = piece // nc
     twin = at(dc=1)
     y_peers = [at(dy=d) for d in range(ny)]
     z_peers = [at(dz=d) for d in range(nz)]
-    blocks = [my_x, left, right, lax.rem(my_x + nx // 2, nx)]
+    owners = [my_x, left, right, lax.rem(my_x + nx // 2, nx)]
+    blocks = [(x, i * piece) for x in owners for i in range(SPLIT)]
     twin_copies, sum_y_copies, sum_z_copies = {}, {}, {}
 
     def multiply(b):
-        at_cols = pl.ds(pl.multiple_of(blocks[b] * cols, cols), cols)
+        x, offset = blocks[b]
+        at_cols = pl.ds(pl.multiple_of(x * cols + offset, piece), piece)
 
         def tile(t, carry):
             at_rows = pl.ds(pl.multiple_of(t * tile_rows, tile_rows), tile_rows)
             units = jnp.concatenate([hidden[e, at_rows, :] for e in range(experts)], axis=1)
-            down = down_out[:, :, at_cols].reshape(experts * hid, cols)
+            down = down_out[:, :, at_cols].reshape(experts * hid, piece)
             val = jnp.dot(units, down, preferred_element_type=f32)
-            val = val.reshape(z_per, ny, r, cols).astype(bf)
-            for c in range(nc):
-                for y in range(ny):
-                    part[b, c, y, pl.ds(t * z_per, z_per)] = val[:, y, :, c * half : (c + 1) * half]
+            val = val.reshape(z_per, ny, r, piece)
+            at_part = pl.ds(pl.multiple_of(t * z_per * r, z_per * r), z_per * r)
+            for y in range(ny):
+                lines = jnp.concatenate([val[z, y] for z in range(z_per)], axis=0).astype(bf)
+                for c in range(nc):
+                    part[b, c, y, at_part, :] = lines[:, c * half : (c + 1) * half]
             return carry
 
         lax.fori_loop(0, tiles, tile, 0)
@@ -331,58 +356,99 @@
             part.at[b, twin[2]], from_twin.at[b], t_send.at[b], t_recv.at[b], twin
         )
 
+    far_y = ny // 2
+    count_y = nz * r
+    halves = (pl.ds(0, count_y // 2), pl.ds(count_y // 2, count_y // 2))
+
+    def to_y_send(b, lane, part_of, landing, target):
+        sum_y_copies[b, lane] = start(
+            part_of, landing, ry_send.at[b, lane], ry_recv.at[b, lane], target
+        )
+
+    def pair_sum(b, y, where):
+        return part[b, my_c, y, where, :] + from_twin[b, y, where, :]
+
     def sum_over_y(b):
         twin_copies[b].wait_recv()
-        for d in range(1, ny):
+        right_y, far, left_y = (y_peers[d][1] for d in (1, far_y, ny - 1))
+        for lane, side in ((0, 1), (1, ny - 1)):
+            to_y[b, far, halves[lane], :] = pair_sum(b, far, halves[lane])
+            to_y_send(
+                b, lane, to_y.at[b, far, halves[lane]], far_in.at[b, lane], y_peers[side]
+            )
+        for lane, side, near_y, where in (
+            (2, 1, right_y, halves[1]),
+            (3, ny - 1, left_y, halves[0]),
+        ):
+            to_y[b, near_y, where, :] = pair_sum(b, near_y, where)
+            to_y_send(
+                b, lane, to_y.at[b, near_y, where], from_y.at[b, lane - 2, where], y_peers[side]
+            )
+
+    def direct_y(b):
+        twin_copies[b].wait_recv()
+        for d in (far_y, 1, ny - 1):
             y = y_peers[d][1]
-            to_y[b, y] = (part[b, my_c, y].astype(f32) + from_twin[b, y].astype(f32)).astype(bf)
-            sum_y_copies[b, d] = start(
-                to_y.at[b, y], from_y.at[b, d], ry_send.at[b, d], ry_recv.at[b, d], y_peers[d]
+            to_y[b, y] = pair_sum(b, y, slice(None))
+            to_y_send(b, d, to_y.at[b, y], from_y.at[b, d - 1], y_peers[d])
+
+    def relay_y(b):
+        right_y, left_y = y_peers[1][1], y_peers[ny - 1][1]
+        for lane, side, near_y, where, came in (
+            (4, 1, right_y, halves[0], 0),
+            (5, ny - 1, left_y, halves[1], 1),
+        ):
+            sum_y_copies[b, came].wait_recv()
+            to_y[b, near_y, where, :] = pair_sum(b, near_y, where) + far_in[b, came]
+            to_y_send(
+                b, lane, to_y.at[b, near_y, where], from_y.at[b, lane - 4, where], y_peers[side]
             )
 
-    def summed(b, z):
-        value = part[b, my_c, my_y, z].astype(f32) + from_twin[b, my_y, z].astype(f32)
-        for d in range(1, ny):
-            value = value + from_y[b, d, z].astype(f32)
-        return value
-
     def sum_over_z(b):
-        for d in range(1, ny):
-            sum_y_copies[b, d].wait_recv()
+        for lane in range(1, ny) if b in DIRECT else range(2, 6):
+            sum_y_copies[b, lane].wait_recv()
+        value = part[b, my_c, my_y].astype(f32) + from_twin[b, my_y].astype(f32)
+        for side in range(ny - 1 if b in DIRECT else 2):
+            value = value + from_y[b, side].astype(f32)
+        value = value.reshape(nz, r, half)
+        of_y[b] = value
+        to_z[b] = value.astype(bf)
         for d in range(1, nz):
-            z = z_peers[d][0]
-            to_z[b, z] = summed(b, z).astype(bf)
             sum_z_copies[b, d] = start(
-                to_z.at[b, z], from_z.at[b, d], rz_send.at[b, d], rz_recv.at[b, d], z_peers[d]
+                to_z.at[b, z_peers[d][0]],
+                from_z.at[b, d],
+                rz_send.at[b, d],
+                rz_recv.at[b, d],
+                z_peers[d],
             )
 
     def finish(b):
-        value = summed(b, my_z)
+        value = of_y[b, my_z]
         for d in range(1, nz):
             sum_z_copies[b, d].wait_recv()
             value = value + from_z[b, d].astype(f32)
         total[b] = value
 
-    multiply(0)
-    d_near[0, 1].wait_recv()
-    multiply(1)
-    sum_over_y(0)
-    d_near[1, 0].wait_recv()
-    multiply(2)
-    sum_over_y(1)
-    sum_over_z(0)
-    sum_over_y(2)
-    for copy in d_far:
-        copy.wait_recv()
-    multiply(3)
-    sum_over_z(1)
-    sum_over_y(3)
-    finish(0)
-    sum_over_z(2)
-    finish(1)
-    sum_over_z(3)
-    finish(2)
-    finish(3)
+    count = len(blocks)
+
+    def first_y(b):
+        (direct_y if b in DIRECT else sum_over_y)(b)
+
+    def second_y(b):
+        if b not in DIRECT:
+            relay_y(b)
+
+    for i in range(count + 5):
+        if i == SPLIT:
+            d_near[0, 1].wait_recv()
+        if i == 2 * SPLIT:
+            d_near[1, 0].wait_recv()
+        if i == 3 * SPLIT:
+            for copy in d_far:
+                copy.wait_recv()
+        for stage, lag in ((multiply, 0), (first_y, 1), (second_y, 2), (sum_over_z, 3), (finish, 5)):
+            if 0 <= i - lag < count:
+                stage(i - lag)
 
     own = mixed_out.shape[0]
     first_core = my_c == 0
@@ -392,12 +458,12 @@
     mine = jnp.where(first_core, low, high)
     swap.wait_recv()
     theirs = last[...]
-    for b, x in enumerate(blocks):
+    for b, (x, offset) in enumerate(blocks):
         pair = [
             jnp.where(first_core, mine[b], theirs[b]),
             jnp.where(first_core, theirs[b], mine[b]),
         ]
-        at_cols = pl.ds(pl.multiple_of(x * cols, cols), cols)
+        at_cols = pl.ds(pl.multiple_of(x * cols + offset, piece), piece)
         mixed_out[:, at_cols] = jnp.concatenate(pair, axis=1).astype(bf)
     for copy in sent:
         copy.wait_send()
@@ -420,7 +486,8 @@
     sub = rows // PARTS
     count = tokens.shape[0]
     r = count // (nz * ny)
-    half = dcols // nc
+    nb = nx * SPLIT
+    half = dcols // nc // SPLIT
     dma = pltpu.SemaphoreType.DMA
     vmem = pl.BlockSpec(memory_space=pltpu.VMEM)
     hbm = pl.BlockSpec(memory_space=pltpu.HBM)
@@ -432,29 +499,34 @@
             pltpu.VMEM((experts, hid, dcols * nx), bf),
             pltpu.VMEM((count // nk, dcols * nx), bf),
         ],
-        in_specs=[hbm, hbm, vmem, hbm, hbm, vmem, vmem],
+        in_specs=[hbm] * 7,
         out_specs=[vmem] * 4,
         scratch_shapes=[
             pltpu.VMEM(gate_weight.shape, f32),
             pltpu.VMEM(up_weight.shape, f32),
             pltpu.VMEM(down_weight.shape, f32),
             pltpu.VMEM(tokens.shape, bf),
+            pltpu.VMEM(gain.shape, f32),
+            pltpu.VMEM(routes.shape, jnp.int32),
+            pltpu.VMEM(logits.shape, f32),
             pltpu.VMEM((2, PARTS, nx, per_x, sub, width), bf),
             pltpu.VMEM((2, PARTS, nk, sub, width), bf),
             pltpu.VMEM((2, PARTS, nz, nyc, sub, width), bf),
             pltpu.VMEM(tokens.shape, bf),
             pltpu.VMEM((experts, count, hid), f32),
             pltpu.VMEM((experts, count, hid), bf),
-            pltpu.VMEM((nx, nc, ny, nz, r, half), bf),
-            pltpu.VMEM((nx, ny, nz, r, half), bf),
-            pltpu.VMEM((nx, ny, nz, r, half), bf),
-            pltpu.VMEM((nx, ny, nz, r, half), bf),
-            pltpu.VMEM((nx, nz, r, half), bf),
-            pltpu.VMEM((nx, nz, r, half), bf),
-            pltpu.VMEM((nx, r, half), f32),
-            pltpu.VMEM((nx, r // nc, half), f32),
-            pltpu.VMEM((nx, r // nc, half), f32),
-            dma((4,)),
+            pltpu.VMEM((nb, nc, ny, nz * r, half), bf),
+            pltpu.VMEM((nb, ny, nz * r, half), bf),
+            pltpu.VMEM((nb, ny, nz * r, half), bf),
+            pltpu.VMEM((nb, ny - 1, nz * r, half), bf),
+            pltpu.VMEM((nb, 2, nz * r // 2, half), bf),
+            pltpu.VMEM((nb, nz, r, half), f32),
+            pltpu.VMEM((nb, nz, r, half), bf),
+            pltpu.VMEM((nb, nz, r, half), bf),
+            pltpu.VMEM((nb, r, half), f32),
+            pltpu.VMEM((nb, r // nc, half), f32),
+            pltpu.VMEM((nb, r // nc, half), f32),
+            dma((7,)),
             dma((2, PARTS, nx)),
             dma((2, PARTS, nx)),
             dma((2, PARTS, nz)),
@@ -465,23 +537,25 @@
             dma((2 * PARTS + 1, 2, 2)),
             dma((2 * PARTS + 1, 2)),
             dma((2 * PARTS + 1, 2)),
-            dma((nx + 1,)),
-            dma((nx + 1,)),
-            dma((nx, ny)),
-            dma((nx, ny)),
-            dma((nx, nz)),
-            dma((nx, nz)),
+            dma((nb + 1,)),
+            dma((nb + 1,)),
+            dma((nb, 6)),
+            dma((nb, 6)),
+            dma((nb, nz)),
+            dma((nb, nz)),
         ],
         compiler_params=pltpu.CompilerParams(
             collective_id=0, has_side_effects=True, vmem_limit_bytes=44 * MIB
         ),
         name="whole",
-    )(*(away(a) for a in (gate_weight, up_weight)), gain, away(down_weight), away(tokens), routes, logits)
-
-
-def write_kernel(a, b, c, a_out, b_out, c_out, sems):
-    pairs = ((a, a_out), (b, b_out), (c, c_out))
-    copies = [pltpu.make_async_copy(src, dst, sems.at[i]) for i, (src, dst) in enumerate(pairs)]
+    )(*(away(a) for a in (gate_weight, up_weight, gain, down_weight, tokens, routes, logits)))
+
+
+def write_kernel(*refs):
+    count = len(refs) // 2
+    copies = [
+        pltpu.make_async_copy(refs[i], refs[count + i], refs[-1].at[i]) for i in range(count)
+    ]
     for copy in copies:
         copy.start()
     for copy in copies:
@@ -505,8 +579,7 @@
         sizes, gate_weight, up_weight, norm_gain[None, :], down_weight, tokens, routes.T, route_logit.T
     )
     full = (gate.shape[0], -1, gate.shape[-1])
-    gate_out, up_out, down_out = write_out(gate.reshape(full), up.reshape(full), down)
-    return (gate_out, up_out, down_out, mixed)
+    return tuple(write_out(gate.reshape(full), up.reshape(full), down, mixed))
 
 
 def solution(mesh):

time: 108 us -> 102 us (0.944)
  Pallas kernels: 105 us -> 102 us
  local copies, waits for them, and re-layouts: 2.66 us -> 0 us
    pallas_call x1, Pallas kernels: 102 us -> 98.8 us  [whole(): pl.pallas_call(functools.partial(whole_kernel, sizes), out_shape=[pltpu.V...]
    unnamed x7 -> x0, local copies, waits for them, and re-layouts: 2.66 us -> none
where the time goes in v4:
time: 102 us
  Pallas kernels  102 us (100%)
    pallas_call x1, Pallas kernels, whole(): pl.pallas_call(functools.partial(whole_kernel, sizes), out_shape=[pltpu.V...  98.8 us
    pallas_call x1, Pallas kernels, write_out(): pl.pallas_call(write_kernel, out_shape=[jax.ShapeDtypeStruct(a.shape, a.d...  2.74 us

profile of v4, /device:TPU:1, one launch (start us, length us, event | category | flops | bytes accessed | tf_op | source)
XLA Modules:
  0.0 102.2 jit_solution(3004212839742025448)
XLA Ops:
  0.6 98.8 %whole.1 = (bf16[4,8,8,32,128]{4,3,2,1,0:T(8,128)(2,1)S(1)}, bf16[4,8,8,32,128]{4,3,2,1,0:T(8,128)(2,1)S(1)}, bf16[4,128,2048]{2,1,0:T(8,128)(2,1)S(1)}, bf16[12,2048]{1,0:T(8,128)(2,1)S(1)}) custom-call(f32[4,32,2048]{2,1,0:T(8,128)} %gate_hbm.1, f32[4,32,2048]{2,1,0:T(8,128)} %up_hbm.1, f32[1,32]{1,0:T(1,128)} %bitcast.9, f32[4,128,512]{2,1,0:T(8,128)} %down_hbm.1, ...), custom_call_target="tpu_custom_call" | custom-call | tf_op jit(solution)/shard_map/whole/pallas_call | solution.py:494
  99.5 2.7 %write_out.1 = (bf16[4,2048,128]{2,1,0:T(8,128)(2,1)}, bf16[4,2048,128]{2,1,0:T(8,128)(2,1)}, bf16[4,128,2048]{2,1,0:T(8,128)(2,1)}, bf16[12,2048]{1,0:T(8,128)(2,1)}) custom-call(bf16[4,2048,128]{2,1,0:T(8,128)(2,1)S(1)} %bitcast.5, bf16[4,2048,128]{2,1,0:T(8,128)(2,1)S(1)} %bitcast.6, bf16[4,128,2048]{2,1,0:T(8,128)(2,1)S(1)} %get-tuple-element.10.refs_2_, ...), custom_call_target="tpu_custom_call" | custom-call | tf_op jit(solution)/shard_map/write_out/pallas_call | solution.py:566

commit v5 on v4

--- a/solution.py
+++ b/solution.py
@@ -14,8 +14,7 @@
 MESH = pl.DeviceIdType.MESH
 MIB = 1024 * 1024
 SPLIT = 1
-DIRECT = ()
-PARTS = 2
+DIRECT = (3,)
 
 
 def whole_kernel(
@@ -41,6 +40,11 @@
     staged,
     spread,
     by_z,
+    staged_b,
+    spread_b,
+    by_z_b,
+    wide,
+    wide_by_z,
     normed,
     share,
     hidden,
@@ -60,6 +64,10 @@
     a_recv,
     z_send,
     z_recv,
+    wz_send,
+    wz_recv,
+    wy_send,
+    wy_recv,
     y_send,
     y_recv,
     c_send,
@@ -130,39 +138,51 @@
 
     rows = gate_in.shape[1]
     width = gate_in.shape[2] // per_x
-    sub = rows // PARTS
     loads[4].wait()
     gain_row = gain_ref[...]
     same = lax.broadcasted_iota(jnp.int32, (rows, rows), 0) == lax.broadcasted_iota(
         jnp.int32, (rows, rows), 1
     )
     gain = jnp.sum(jnp.where(same, gain_row, 0.0), axis=1, keepdims=True)
-    chunks = [(m, h) for m in (0, 1) for h in range(PARTS)]
+    step_a, step_b = rows // 2, rows // 4
+    chunks = [
+        (0, 0, step_a),
+        (0, step_a, step_a),
+        (1, 0, step_a),
+        (1, step_a, step_b),
+        (1, step_a + step_b, step_b),
+    ]
+    stages = [(staged.at[i], spread.at[i], by_z.at[i]) for i in range(3)]
+    stages.append((staged_b, spread_b, by_z_b))
 
     a_copies = {}
-    for m, ref in ((0, gate_in), (1, up_in)):
-        loads[m].wait()
-        for h in range(PARTS):
-            lo = h * sub
-            for d in range(nx):
-                expert = lax.rem(my_x + d, nx)
-                for k in range(per_x):
-                    block = ref[expert, lo : lo + sub, k * width : (k + 1) * width]
-                    block = (block * gain[lo : lo + sub]).astype(bf)
-                    if d == 0:
-                        spread[m, h, my_x * per_x + k] = block
-                    else:
-                        staged[m, h, d, k] = block
-            if m + h == 0:
-                pl.semaphore_wait(barrier, len(peers))
-            for d in range(1, nx):
-                a_copies[m, h, d] = start(
-                    staged.at[m, h, d],
-                    spread.at[m, h, pl.ds(my_x * per_x, per_x)],
-                    a_send.at[m, h, d],
-                    a_recv.at[m, h, d],
-                    at(dx=d),
-                )
+    for q, (m, lo, n) in enumerate(chunks):
+        ref = (gate_in, up_in)[m]
+        if lo == 0:
+            loads[m].wait()
+        for d in range(nx):
+            expert = lax.rem(my_x + d, nx)
+            for k in range(per_x):
+                block = ref[expert, lo : lo + n, k * width : (k + 1) * width]
+                block = (block * gain[lo : lo + n]).astype(bf)
+                if q == len(chunks) - 1:
+                    wide[expert, my_x * per_x + k] = block
+                elif d == 0:
+                    stages[q][1][my_x * per_x + k] = block
+                else:
+                    stages[q][0][d, k] = block
+        if q == 0:
+            pl.semaphore_wait(barrier, len(peers))
+        if q == len(chunks) - 1:
+            continue
+        for d in range(1, nx):
+            a_copies[q, d] = start(
+                stages[q][0].at[d],
+                stages[q][1].at[pl.ds(my_x * per_x, per_x)],
+                a_send.at[q, d],
+                a_recv.at[q, d],
+                at(dx=d),
+            )
 
     cols = down_in.shape[2]
     half_e = nx // 2
@@ -190,12 +210,18 @@
             pl.ds(h * half_e, half_e), :, pl.ds(pl.multiple_of(x * cols, cols), cols)
         ]
 
-    d_tag = len(chunks)
-    d_near = {}
-    for s in (0, 1):
-        d_near[s, s] = near(d_tag, down_block, s, s)
-    for s in (0, 1):
-        d_near[s, 1 - s] = near(d_tag, down_block, s, 1 - s)
+    def near_all(tag, block):
+        copies = {(s, s): near(tag, block, s, s) for s in (0, 1)}
+        copies.update({(s, 1 - s): near(tag, block, s, 1 - s) for s in (0, 1)})
+        return copies
+
+    def wide_block(x, h):
+        return wide.at[
+            pl.ds(h * half_e, half_e), pl.ds(pl.multiple_of(x * per_x, per_x), per_x)
+        ]
+
+    w_tag, d_tag = len(chunks) - 1, len(chunks)
+    w_near = near_all(w_tag, wide_block)
 
     loads[3].wait()
     step = 48
@@ -225,42 +251,42 @@
     half_z = nz // 2
 
     def over_z(q):
-        m, h = q
+        _, by_x, by_z_q = stages[q]
         for d in range(1, nx):
-            a_copies[m, h, d].wait_recv()
+            a_copies[q, d].wait_recv()
         for dz in range(1, nz):
             peer = at(dz=dz)
             z_copies[q, dz] = start(
-                spread.at[m, h, pl.ds(peer[0] * nyc, nyc)],
-                by_z.at[m, h, my_z],
-                z_send.at[m, h, dz],
-                z_recv.at[m, h, dz],
+                by_x.at[pl.ds(peer[0] * nyc, nyc)],
+                by_z_q.at[my_z],
+                z_send.at[q, dz],
+                z_recv.at[q, dz],
                 peer,
             )
-        by_z[m, h, my_z] = spread[m, h, pl.ds(my_z * nyc, nyc)]
+        by_z_q[my_z] = by_x[pl.ds(my_z * nyc, nyc)]
 
     def over_yc(q):
-        m, h = q
-        out, lo = outs[m], h * sub
+        m, lo, n = chunks[q]
+        out, by_z_q = outs[m], stages[q][2]
         for dz in range(1, nz):
             z_copies[q, dz].wait_recv()
         for i, (dy, dc) in enumerate(yc_steps):
             peer = at(dy=dy, dc=dc)
             y_copies[q, i] = start(
-                by_z.at[m, h, :, peer[1] * nc + peer[2]],
-                out.at[my_x, :, my_yc, pl.ds(lo, sub)],
-                y_send.at[m, h, i],
-                y_recv.at[m, h, i],
+                by_z_q.at[:, peer[1] * nc + peer[2]],
+                out.at[my_x, :, my_yc, pl.ds(lo, n)],
+                y_send.at[q, i],
+                y_recv.at[q, i],
                 peer,
             )
-        out[my_x, :, my_yc, lo : lo + sub, :] = by_z[m, h, :, my_yc]
+        out[my_x, :, my_yc, lo : lo + n, :] = by_z_q[:, my_yc]
 
     def out_block(q):
-        m, h = q
-        return lambda x, half: outs[m].at[x, pl.ds(half * half_z, half_z), :, pl.ds(h * sub, sub)]
+        m, lo, n = chunks[q]
+        return lambda x, half: outs[m].at[x, pl.ds(half * half_z, half_z), :, pl.ds(lo, n)]
 
     def over_x(q):
-        tag = chunks.index(q)
+        tag = q
         for i in range(len(yc_steps)):
             y_copies[q, i].wait_recv()
         for s in (0, 1):
@@ -271,7 +297,7 @@
     def onward(q):
         for s in (0, 1):
             c_near[q, s, s].wait_recv()
-            c_far[q, s] = pass_on(chunks.index(q), out_block(q), s)
+            c_far[q, s] = pass_on(q, out_block(q), s)
 
     experts = nx
     hid = width
@@ -294,36 +320,90 @@
 
         lax.fori_loop(0, tiles, tile, 0)
 
-    q0, q1, q2, q3 = chunks
-    over_z(q0)
-    over_z(q1)
-    over_z(q2)
-    over_yc(q0)
-    over_z(q3)
-    over_x(q0)
-    over_yc(q1)
-    onward(q0)
-    over_x(q1)
-    over_yc(q2)
-    onward(q1)
-    over_x(q2)
-    over_yc(q3)
-    onward(q2)
-    over_x(q3)
-    run_expert(my_x)
-    onward(q3)
+    order = [my_x, left, right, lax.rem(my_x + nx // 2, nx)]
+    w_out, w_lo, sub = outs[chunks[-1][0]], chunks[-1][1], chunks[-1][2]
+    wz_copies, wy_copies = {}, {}
+
+    def wide_over_z():
+        for s in (0, 1):
+            w_near[s, 1 - s].wait_recv()
+        for copy in w_onward:
+            copy.wait_recv()
+        for i, e in enumerate(order):
+            for dz in range(1, nz):
+                peer = at(dz=dz)
+                wz_copies[i, dz] = start(
+                    wide.at[e, pl.ds(peer[0] * nyc, nyc)],
+                    wide_by_z.at[e, my_z],
+                    wz_send.at[i, dz],
+                    wz_recv.at[i, dz],
+                    peer,
+                )
+            wide_by_z[e, my_z] = wide[e, pl.ds(my_z * nyc, nyc)]
+
+    def wide_over_yc(i):
+        e = order[i]
+        for dz in range(1, nz):
+            wz_copies[i, dz].wait_recv()
+        for j, (dy, dc) in enumerate(yc_steps):
+            peer = at(dy=dy, dc=dc)
+            wy_copies[i, j] = start(
+                wide_by_z.at[e, :, peer[1] * nc + peer[2]],
+                w_out.at[e, :, my_yc, pl.ds(w_lo, sub)],
+                wy_send.at[i, j],
+                wy_recv.at[i, j],
+                peer,
+            )
+        w_out[e, :, my_yc, w_lo : w_lo + sub, :] = wide_by_z[e, :, my_yc]
+
+    def wide_done(i):
+        for j in range(len(yc_steps)):
+            wy_copies[i, j].wait_recv()
+
+    over_z(0)
+    over_z(1)
+    over_z(2)
+    over_yc(0)
+    over_z(3)
+    w_onward = []
+    for s in (0, 1):
+        w_near[s, s].wait_recv()
+        w_onward.append(pass_on(w_tag, wide_block, s))
+    d_near = {(s, s): near(d_tag, down_block, s, s) for s in (0, 1)}
+    over_x(0)
+    over_yc(1)
+    wide_over_z()
+    over_yc(2)
+    over_x(1)
+    onward(0)
+    over_yc(3)
+    over_x(2)
+    wide_over_yc(0)
+    over_x(3)
+    onward(1)
+    wide_over_yc(1)
+    wide_done(0)
+    run_expert(order[0])
+    wide_over_yc(2)
+    wide_over_yc(3)
+    onward(2)
+    onward(3)
+    for s in (0, 1):
+        d_near[s, 1 - s] = near(d_tag, down_block, s, 1 - s)
     d_far = []
     for s in (0, 1):
         d_near[s, s].wait_recv()
         d_far.append(pass_on(d_tag, down_block, s))
-    for s, e in ((0, left), (1, right)):
-        for q in chunks:
+    for i, s in ((1, 0), (2, 1)):
+        wide_done(i)
+        for q in range(4):
             c_near[q, s, 1 - s].wait_recv()
-        run_expert(e)
-    for q in chunks:
+        run_expert(order[i])
+    wide_done(3)
+    for q in range(4):
         for s in (0, 1):
             c_far[q, s].wait_recv()
-    run_expert(lax.rem(my_x + nx // 2, nx))
+    run_expert(order[3])
 
     piece = cols // SPLIT
     half = piece // nc
@@ -429,8 +509,6 @@
             value = value + from_z[b, d].astype(f32)
         total[b] = value
 
-    count = len(blocks)
-
     def first_y(b):
         (direct_y if b in DIRECT else sum_over_y)(b)
 
@@ -438,17 +516,39 @@
         if b not in DIRECT:
             relay_y(b)
 
-    for i in range(count + 5):
-        if i == SPLIT:
-            d_near[0, 1].wait_recv()
-        if i == 2 * SPLIT:
-            d_near[1, 0].wait_recv()
-        if i == 3 * SPLIT:
-            for copy in d_far:
-                copy.wait_recv()
-        for stage, lag in ((multiply, 0), (first_y, 1), (second_y, 2), (sum_over_z, 3), (finish, 5)):
-            if 0 <= i - lag < count:
-                stage(i - lag)
+    def wait_left():
+        d_near[0, 1].wait_recv()
+
+    def wait_right():
+        d_near[1, 0].wait_recv()
+
+    def wait_far():
+        for copy in d_far:
+            copy.wait_recv()
+
+    multiply(0)
+    first_y(0)
+    wait_left()
+    multiply(1)
+    first_y(1)
+    second_y(0)
+    wait_right()
+    multiply(2)
+    first_y(2)
+    second_y(1)
+    sum_over_z(0)
+    wait_far()
+    multiply(3)
+    second_y(2)
+    first_y(3)
+    sum_over_z(1)
+    second_y(3)
+    finish(0)
+    sum_over_z(2)
+    finish(1)
+    sum_over_z(3)
+    finish(2)
+    finish(3)
 
     own = mixed_out.shape[0]
     first_core = my_c == 0
@@ -483,7 +583,6 @@
     hid, dcols = down_weight.shape[1:]
     bf, f32 = jnp.bfloat16, jnp.float32
     steps = nyc - 1
-    sub = rows // PARTS
     count = tokens.shape[0]
     r = count // (nz * ny)
     nb = nx * SPLIT
@@ -509,9 +608,14 @@
             pltpu.VMEM(gain.shape, f32),
             pltpu.VMEM(routes.shape, jnp.int32),
             pltpu.VMEM(logits.shape, f32),
-            pltpu.VMEM((2, PARTS, nx, per_x, sub, width), bf),
-            pltpu.VMEM((2, PARTS, nk, sub, width), bf),
-            pltpu.VMEM((2, PARTS, nz, nyc, sub, width), bf),
+            pltpu.VMEM((3, nx, per_x, rows // 2, width), bf),
+            pltpu.VMEM((3, nk, rows // 2, width), bf),
+            pltpu.VMEM((3, nz, nyc, rows // 2, width), bf),
+            pltpu.VMEM((nx, per_x, rows // 4, width), bf),
+            pltpu.VMEM((nk, rows // 4, width), bf),
+            pltpu.VMEM((nz, nyc, rows // 4, width), bf),
+            pltpu.VMEM((nx, nk, rows // 4, width), bf),
+            pltpu.VMEM((nx, nz, nyc, rows // 4, width), bf),
             pltpu.VMEM(tokens.shape, bf),
             pltpu.VMEM((experts, count, hid), f32),
             pltpu.VMEM((experts, count, hid), bf),
@@ -527,16 +631,20 @@
             pltpu.VMEM((nb, r // nc, half), f32),
             pltpu.VMEM((nb, r // nc, half), f32),
             dma((7,)),
-            dma((2, PARTS, nx)),
-            dma((2, PARTS, nx)),
-            dma((2, PARTS, nz)),
-            dma((2, PARTS, nz)),
-            dma((2, PARTS, steps)),
-            dma((2, PARTS, steps)),
-            dma((2 * PARTS + 1, 2, 2)),
-            dma((2 * PARTS + 1, 2, 2)),
-            dma((2 * PARTS + 1, 2)),
-            dma((2 * PARTS + 1, 2)),
+            dma((4, nx)),
+            dma((4, nx)),
+            dma((4, nz)),
+            dma((4, nz)),
+            dma((nx, nz)),
+            dma((nx, nz)),
+            dma((nx, steps)),
+            dma((nx, steps)),
+            dma((4, steps)),
+            dma((4, steps)),
+            dma((6, 2, 2)),
+            dma((6, 2, 2)),
+            dma((6, 2)),
+            dma((6, 2)),
             dma((nb + 1,)),
             dma((nb + 1,)),
             dma((nb, 6)),

time: 102 us -> 102 us (level)
  no operation moved by 1% of the time
where the time goes in v5:
time: 102 us; the launch traced here: 101 us
  Pallas kernels  101 us (99%)
    pallas_call x1, Pallas kernels, whole(): pl.pallas_call(functools.partial(whole_kernel, sizes), out_shape=[pltpu.V...  98 us
    pallas_call x1, Pallas kernels, write_out(): pl.pallas_call(write_kernel, out_shape=[jax.ShapeDtypeStruct(a.shape, a.d...  2.74 us

profile of v5, /device:TPU:1, one launch (start us, length us, event | category | flops | bytes accessed | tf_op | source)
XLA Modules:
  0.0 101.4 jit_solution(9107547100242687390)
XLA Ops:
  0.6 98.0 %whole.1 = (bf16[4,8,8,32,128]{4,3,2,1,0:T(8,128)(2,1)S(1)}, bf16[4,8,8,32,128]{4,3,2,1,0:T(8,128)(2,1)S(1)}, bf16[4,128,2048]{2,1,0:T(8,128)(2,1)S(1)}, bf16[12,2048]{1,0:T(8,128)(2,1)S(1)}) custom-call(f32[4,32,2048]{2,1,0:T(8,128)} %gate_hbm.1, f32[4,32,2048]{2,1,0:T(8,128)} %up_hbm.1, f32[1,32]{1,0:T(1,128)} %bitcast.9, f32[4,128,512]{2,1,0:T(8,128)} %down_hbm.1, ...), custom_call_target="tpu_custom_call" | custom-call | tf_op jit(solution)/shard_map/whole/pallas_call | solution.py:593
  98.7 2.7 %write_out.1 = (bf16[4,2048,128]{2,1,0:T(8,128)(2,1)}, bf16[4,2048,128]{2,1,0:T(8,128)(2,1)}, bf16[4,128,2048]{2,1,0:T(8,128)(2,1)}, bf16[12,2048]{1,0:T(8,128)(2,1)}) custom-call(bf16[4,2048,128]{2,1,0:T(8,128)(2,1)S(1)} %bitcast.5, bf16[4,2048,128]{2,1,0:T(8,128)(2,1)S(1)} %bitcast.6, bf16[4,128,2048]{2,1,0:T(8,128)(2,1)S(1)} %get-tuple-element.10.refs_2_, ...), custom_call_target="tpu_custom_call" | custom-call | tf_op jit(solution)/shard_map/write_out/pallas_call | solution.py:674

commit v6 on v5

--- a/solution.py
+++ b/solution.py
@@ -405,6 +405,7 @@
             c_far[q, s].wait_recv()
     run_expert(order[3])
 
+    early = len(sent) - 2
     piece = cols // SPLIT
     half = piece // nc
     twin = at(dc=1)
@@ -537,6 +538,9 @@
     first_y(2)
     second_y(1)
     sum_over_z(0)
+    for copy in sent[:early]:
+        copy.wait_send()
+    del sent[:early]
     wait_far()
     multiply(3)
     second_y(2)

time: 102 us -> 101 us (level)
  no operation moved by 1% of the time
where the time goes in v6:
time: 101 us
  Pallas kernels  101 us (100%)
    pallas_call x1, Pallas kernels, whole(): pl.pallas_call(functools.partial(whole_kernel, sizes), out_shape=[pltpu.V...  97.9 us
    pallas_call x1, Pallas kernels, write_out(): pl.pallas_call(write_kernel, out_shape=[jax.ShapeDtypeStruct(a.shape, a.d...  2.74 us

profile of v6, /device:TPU:1, one launch (start us, length us, event | category | flops | bytes accessed | tf_op | source)
XLA Modules:
  0.0 101.3 jit_solution(16152510258040118242)
XLA Ops:
  0.6 97.9 %whole.1 = (bf16[4,8,8,32,128]{4,3,2,1,0:T(8,128)(2,1)S(1)}, bf16[4,8,8,32,128]{4,3,2,1,0:T(8,128)(2,1)S(1)}, bf16[4,128,2048]{2,1,0:T(8,128)(2,1)S(1)}, bf16[12,2048]{1,0:T(8,128)(2,1)S(1)}) custom-call(f32[4,32,2048]{2,1,0:T(8,128)} %gate_hbm.1, f32[4,32,2048]{2,1,0:T(8,128)} %up_hbm.1, f32[1,32]{1,0:T(1,128)} %bitcast.9, f32[4,128,512]{2,1,0:T(8,128)} %down_hbm.1, ...), custom_call_target="tpu_custom_call" | custom-call | tf_op jit(solution)/shard_map/whole/pallas_call | solution.py:597
  98.5 2.7 %write_out.1 = (bf16[4,2048,128]{2,1,0:T(8,128)(2,1)}, bf16[4,2048,128]{2,1,0:T(8,128)(2,1)}, bf16[4,128,2048]{2,1,0:T(8,128)(2,1)}, bf16[12,2048]{1,0:T(8,128)(2,1)}) custom-call(bf16[4,2048,128]{2,1,0:T(8,128)(2,1)S(1)} %bitcast.5, bf16[4,2048,128]{2,1,0:T(8,128)(2,1)S(1)} %bitcast.6, bf16[4,128,2048]{2,1,0:T(8,128)(2,1)S(1)} %get-tuple-element.10.refs_2_, ...), custom_call_target="tpu_custom_call" | custom-call | tf_op jit(solution)/shard_map/write_out/pallas_call | solution.py:678
